TPU v7x, 256 devices: a whole 4x4x8 slice. The times are simulated.
256 devices in a mesh: sp: 64 (over z, x, core), tp: 4 (over y).
Axes of the slice: x: 4, y: 4, z: 8, core: 2. Of those that a mesh axis runs over, the one named last changes fastest.
Arguments:
- stream_in: bfloat16 [16384, 2048], P(('sp', 'tp')), may hold values from -6 to 6
- queries: bfloat16 [16384, 1024], P('sp', 'tp'), may hold values from -48 to 48
- keys: bfloat16 [16384, 512], P('sp', 'tp'), may hold values from -48 to 48
- values: bfloat16 [16384, 512], P('sp', 'tp'), may hold values from -6 to 6
- query_gain: float32 [64], replicated, may hold values from 1.5 to 6
- key_gain: float32 [64], replicated, may hold values from 1.5 to 6
- out_rows: bfloat16 [1024, 2048], P('tp'), may hold values from -0.1875 to 0.1875
- norm_gain: float32 [2048], replicated, may hold values from 0.1 to 1.9
- route_ids: int32 [16384, 2], P(('sp', 'tp')), may hold values from 0 to 63, all different within a row; in each aligned block of 64 rows (0 to 63, 64 to 127, ...) at most 3 rows name the same one
- route_weights: float32 [16384, 2], P(('sp', 'tp')), may hold values from 0.25 to 1
- gate_weight: bfloat16 [64, 2048, 3072], P('sp', None, 'tp'), may hold values from -0.125 to 0.125
- up_weight: bfloat16 [64, 2048, 3072], P('sp', None, 'tp'), may hold values from -0.125 to 0.125
- down_weight: bfloat16 [64, 3072, 2048], P('sp', 'tp'), may hold values from -0.109375 to 0.109375
Outputs:
- stream_out: bfloat16 [16384, 2048], P(('sp', 'tp'))
Inputs may be any that keep to these rules, and one draw needn't show every extreme that they name: `route_ids`: each row names 2 different experts; among the rows of one device no expert is named more than 3 times.
All inputs are finite; a program needn't handle non-finite values.
Results may differ from a plain program's by a relative error of at most 0.014.
The roundings to bfloat16 on the way count: a program that leaves them out, or rounds other values in their place, can miss the bound.
Values may be sent and summed in bfloat16 or wider, within the bound.
A program may use at most 128 MiB of HBM per device.

v0:
```python
import math

import jax
import jax.numpy as jnp
from jax import lax
from jax.sharding import PartitionSpec as P

GRID_W = 64


EPS = 1e-06
THETA = 10000.0


def partner(x, axis, distance):
    return lax.ppermute(x, axis, [(i, i ^ 1 << distance) for i in range(lax.axis_size(axis))])


def grouped_exchange(x, axis, split_dim, concat_dim, work, item_dim, out_dim):
    items = jax.tree.leaves(x)[0].shape[item_dim]
    count = 2 if items % 2 == 0 else 1
    outs = []
    for k in range(count):
        group = jax.tree.map(
            lambda a: lax.slice_in_dim(
                a, k * (items // count), (k + 1) * (items // count), axis=item_dim
            ),
            x,
        )
        outs.append(
            work(
                lax.all_to_all(
                    group, axis, split_axis=split_dim, concat_axis=concat_dim, tiled=True
                )
            )
        )
    return jax.tree.map(lambda *parts: jnp.concatenate(parts, axis=out_dim), *outs)


def turn_tables(offset, count, head_size):
    position = offset + jnp.arange(count, dtype=jnp.int32)
    grid_row = (position // GRID_W).astype(jnp.float32)
    column = (position % GRID_W).astype(jnp.float32)
    pair_index = jnp.arange(head_size // 4, dtype=jnp.float32)
    inverse = THETA ** (-4.0 * pair_index / head_size)
    angles = jnp.concatenate([grid_row[:, None] * inverse, column[:, None] * inverse], axis=1)
    return (jnp.cos(angles), jnp.sin(angles))


def normalize_rotate(block_data, gain_vector, cos_table, sin_table):
    row_count = block_data.shape[0]
    head_size = gain_vector.shape[0]
    wide = block_data.astype(jnp.float32).reshape(row_count, -1, head_size)
    wide = wide * lax.rsqrt(jnp.mean(wide * wide, axis=-1, keepdims=True) + EPS) * gain_vector
    pairs = wide.reshape(row_count, wide.shape[1], head_size // 2, 2)
    even_part = pairs[..., 0]
    odd_part = pairs[..., 1]
    cosine = cos_table[:, None, :]
    sine_part = sin_table[:, None, :]
    turned = jnp.stack(
        [even_part * cosine - odd_part * sine_part, even_part * sine_part + odd_part * cosine],
        axis=-1,
    )
    return turned.reshape(row_count, -1).astype(jnp.bfloat16)


def local(
    stream_in,
    queries,
    keys,
    values,
    query_gain,
    key_gain,
    out_rows,
    norm_gain,
    route_ids,
    route_weights,
    gate_weight,
    up_weight,
    down_weight,
):
    head_size = query_gain.shape[0]
    seq_rows = queries.shape[0]
    query_heads = queries.shape[1] // head_size
    key_heads = keys.shape[1] // head_size
    group_head_count = query_heads // key_heads
    whole_out = lax.all_gather(out_rows, "tp", axis=0, tiled=True)
    place_in_seq = lax.axis_index("sp")
    cos_table, sin_table = turn_tables(place_in_seq * seq_rows, seq_rows, head_size)
    rotated_queries = normalize_rotate(queries, query_gain, cos_table, sin_table).reshape(
        seq_rows, key_heads, group_head_count, head_size
    )
    rotated_keys = normalize_rotate(keys, key_gain, cos_table, sin_table)
    score_scale = head_size ** (-0.5)

    def absorb(carry, pieces):
        key_piece, value_piece = pieces
        sequence_length = key_piece.shape[0]
        span_rows = math.gcd(sequence_length, 4 * seq_rows)
        block_count = sequence_length // span_rows
        key_blocks = key_piece.reshape(block_count, span_rows, key_heads, head_size)
        value_blocks = value_piece.reshape(block_count, span_rows, key_heads, head_size)

        def one_block(running, blocks_pair):
            row_top, row_total, weighted = running
            key_block, value_block = blocks_pair
            scores = (
                jnp.einsum(
                    "qkgd,skd->qkgs", rotated_queries, key_block, preferred_element_type=jnp.float32
                )
                * score_scale
            )
            new_top = jnp.maximum(row_top, jnp.max(scores, axis=-1))
            weights = jnp.exp(scores - new_top[..., None])
            shrink = jnp.exp(row_top - new_top)
            row_total = row_total * shrink + jnp.sum(weights, axis=-1)
            weighted = weighted * shrink[..., None] + jnp.einsum(
                "qkgs,skd->qkgd",
                weights.astype(jnp.bfloat16),
                value_block,
                preferred_element_type=jnp.float32,
            )
            return ((new_top, row_total, weighted), None)

        return lax.scan(one_block, carry, (key_blocks, value_blocks))[0]

    start_top = jnp.full((seq_rows, key_heads, group_head_count), -1e30, jnp.float32)
    start_total = jnp.zeros((seq_rows, key_heads, group_head_count), jnp.float32)
    start_weighted = jnp.zeros((seq_rows, key_heads, group_head_count, head_size), jnp.float32)
    carried = absorb((start_top, start_total, start_weighted), (rotated_keys, values))
    held_keys = rotated_keys
    held_values = values
    level_count = lax.axis_size("sp").bit_length() - 1
    for bit in range(level_count):
        partner_keys, partner_values = partner((held_keys, held_values), "sp", bit)
        carried = absorb(carried, (partner_keys, partner_values))
        if bit + 1 < level_count:
            held_keys = jnp.concatenate([held_keys, partner_keys], axis=0)
            held_values = jnp.concatenate([held_values, partner_values], axis=0)
    row_top, row_total, weighted = carried
    attended = (
        (weighted / row_total[..., None])
        .astype(jnp.bfloat16)
        .reshape(seq_rows, query_heads * head_size)
    )
    token_heads = lax.all_to_all(attended, "tp", split_axis=0, concat_axis=1, tiled=True)
    projected = jnp.dot(token_heads, whole_out, preferred_element_type=jnp.float32)
    stream = (stream_in.astype(jnp.float32) + projected).astype(jnp.bfloat16)
    stream_wide = stream.astype(jnp.float32)
    normed = (
        stream_wide
        * lax.rsqrt(jnp.mean(stream_wide * stream_wide, axis=1, keepdims=True) + EPS)
        * norm_gain
    ).astype(jnp.bfloat16)
    tokens = stream.shape[0]
    model_width = stream.shape[1]
    top_count = route_ids.shape[1]
    experts = lax.axis_size("sp")
    routed = tokens * top_count
    capacity = max(2, (5 * routed + 4 * experts - 1) // (4 * experts))
    flat_ids = route_ids.reshape(routed)
    member = (flat_ids[:, None] == jnp.arange(experts, dtype=jnp.int32)[None, :]).astype(jnp.int32)
    earlier = jnp.cumsum(member, axis=0) - member
    slot_rank = jnp.sum(earlier * member, axis=1)
    target = flat_ids * capacity + slot_rank
    placed = (target[:, None] == jnp.arange(experts * capacity, dtype=jnp.int32)[None, :]).astype(
        jnp.bfloat16
    )
    placed = placed.reshape(tokens, top_count, experts * capacity)
    outgoing = jnp.einsum("tks,td->sd", placed, normed, preferred_element_type=jnp.float32).astype(
        jnp.bfloat16
    )
    outgoing = outgoing.reshape(experts, capacity, model_width)
    gate_shard = gate_weight[0]
    up_shard = up_weight[0]
    down_shard = down_weight[0]

    def expert_work(arrived):
        sources, slot_count, width_here = arrived.shape
        flat_rows = arrived.reshape(sources * slot_count, width_here)
        row_piece = lax.all_gather(flat_rows, "tp", axis=0, tiled=True)
        gate_value = jnp.dot(row_piece, gate_shard, preferred_element_type=jnp.float32)
        up_value = jnp.dot(row_piece, up_shard, preferred_element_type=jnp.float32)
        hidden = (jax.nn.silu(gate_value) * up_value).astype(jnp.bfloat16)
        summed = lax.psum_scatter(
            jnp.dot(
                lax.slice_in_dim(hidden, 0, sources * slot_count * lax.axis_size("tp"), axis=0),
                down_shard,
                preferred_element_type=jnp.float32,
            ).astype(jnp.bfloat16),
            "tp",
            scatter_dimension=0,
            tiled=True,
        )
        answer = summed.reshape(sources, slot_count, width_here)
        return lax.all_to_all(answer, "sp", split_axis=0, concat_axis=0, tiled=True)

    returned = grouped_exchange(outgoing, "sp", 0, 0, expert_work, 1, 1)
    expert_back = returned.reshape(experts * capacity, model_width)
    picked = jnp.einsum("tks,sd->tkd", placed, expert_back, preferred_element_type=jnp.float32)
    mixed_out = stream_wide + jnp.sum(route_weights[:, :, None] * picked, axis=1)
    return mixed_out.astype(jnp.bfloat16)


def solution(mesh):
    return jax.shard_map(
        local,
        mesh=mesh,
        in_specs=(
            P(("sp", "tp"), None),
            P("sp", "tp"),
            P("sp", "tp"),
            P("sp", "tp"),
            P(),
            P(),
            P("tp", None),
            P(),
            P(("sp", "tp"), None),
            P(("sp", "tp"), None),
            P("sp", None, "tp"),
            P("sp", None, "tp"),
            P("sp", "tp", None),
        ),
        out_specs=P(("sp", "tp"), None),
        check_vma=False,
    )
```

profile of v0, /device:TPU:33, one launch (start us, length us, event | category | flops | bytes accessed | tf_op | source)
XLA Modules:
  0.0 645.2 jit_solution(744757202785638066)
XLA Ops:
  21.1 2.3 fusion.122
  35.2 2.7 collective-permute-start.2
  48.7 2.2 pad_maximum_fusion
  57.8 1.9 constant_dynamic-update-slice_fusion.12
  61.4 3.1 fusion.80
  64.5 2.2 reshape.298
  66.8 2.0 copy.102
  68.7 5.8 collective-permute-done.7
  74.6 3.2 reshape.324
  77.8 3.5 copy.103
  81.3 2.1 constant_dynamic-update-slice_fusion.11
  83.4 2.8 collective-permute-start.8
  86.2 2.2 constant_dynamic-update-slice_fusion.17
  88.4 7.3 %while.6 = (s32[]{:T(128)}, f32[256,2,2]{0,2,1:T(2,128)S(1)}, f32[256,2,2]{0,2,1:T(2,128)S(1)}, f32[256,2,2,64]{0,3,2,1:T(8,128)S(1)}, bf16[2,1024,2,64]{1,3,2,0...) while((s32[]{:T(128)}, f32[256,2,2]{0,2,1:T(2,128)S(1)}, ...), condition=%wide.region_13.14_spmd, body=%wide.region_10.13_spmd.sunk | while | flops 276957184 | bytes 15925377 | solution.py:125
  95.7 58.6 %collective-permute-done.8 = bf16[4096,128]{0,1:T(8,128)(2,1)} collective-permute-done((bf16[4096,128]{0,1:T(8,128)(2,1)}, bf16[4096,128]{0,1:T(8,128)(2,1)}, u32[]{:S(2)}, u32[]{:S(2)}) %collective-permute-start.8) | collective-permute-done | bytes 1048608 | tf_op jit(solution)/shard_map/ppermute | solution.py:16
  154.3 2.6 reshape.300
  156.9 2.5 copy.105
  159.4 17.3 %collective-permute-done.9 = bf16[4096,128]{1,0:T(8,128)(2,1)} collective-permute-done((bf16[4096,128]{1,0:T(8,128)(2,1)}, bf16[4096,128]{1,0:T(8,128)(2,1)}, u32[]{:S(2)}, u32[]{:S(2)}) %collective-permute-start.9) | collective-permute-done | bytes 1048608 | tf_op jit(solution)/shard_map/ppermute | solution.py:16
  176.7 5.0 reshape.325
  181.7 5.9 copy.106
  187.6 2.3 constant_dynamic-update-slice_fusion.10
  189.9 3.8 collective-permute-start.10
  193.7 2.3 constant_dynamic-update-slice_fusion.16
  197.7 17.3 %while.7 = (s32[]{:T(128)}, f32[256,2,2]{0,2,1:T(2,128)S(1)}, f32[256,2,2]{0,2,1:T(2,128)S(1)}, f32[256,2,2,64]{0,3,2,1:T(8,128)S(1)}, bf16[4,1024,2,64]{1,3,2,0...) while((s32[]{:T(128)}, f32[256,2,2]{0,2,1:T(2,128)S(1)}, ...), condition=%wide.region_17.18_spmd, body=%wide.region_14.17_spmd.sunk | while | flops 276957184 | bytes 13828197 | solution.py:125
  200.2 1.8 fusion.167
  204.5 1.8 fusion.167
  208.8 1.8 fusion.167
  215.0 37.2 %collective-permute-done.10 = bf16[8192,128]{0,1:T(8,128)(2,1)} collective-permute-done((bf16[8192,128]{0,1:T(8,128)(2,1)}, bf16[8192,128]{0,1:T(8,128)(2,1)}, u32[]{:S(2)}, u32[]{:S(2)}) %collective-permute-start.10) | collective-permute-done | bytes 2097184 | tf_op jit(solution)/shard_map/ppermute | solution.py:16
  252.2 3.0 copy.143
  255.2 2.5 copy.108
  257.6 55.7 %collective-permute-done.11 = bf16[8192,128]{1,0:T(8,128)(2,1)} collective-permute-done((bf16[8192,128]{1,0:T(8,128)(2,1)}, bf16[8192,128]{1,0:T(8,128)(2,1)}, u32[]{:S(2)}, u32[]{:S(2)}) %collective-permute-start.11) | collective-permute-done | bytes 2097184 | tf_op jit(solution)/shard_map/ppermute | solution.py:16
  313.3 8.3 %reshape.326 = bf16[8,1024,2,64]{3,2,1,0:T(2,128)(2,1)} reshape(bf16[8192,128]{1,0:T(8,128)(2,1)} %collective-permute-done.11) | data formatting | bytes 4194304 | tf_op jit(solution)/shard_map/reshape | solution.py:102
  321.6 10.7 %copy.109 = bf16[8,1024,2,64]{1,3,2,0:T(8,128)(2,1)} copy(bf16[8,1024,2,64]{3,2,1,0:T(2,128)(2,1)} %reshape.326) | data formatting | bytes 4194304 | tf_op jit(solution)/shard_map/while | solution.py:125
  332.3 34.5 %while.8 = (s32[]{:T(128)}, f32[256,2,2]{0,2,1:T(2,128)S(1)}, f32[256,2,2]{0,2,1:T(2,128)S(1)}, f32[256,2,2,64]{0,3,2,1:T(8,128)S(1)}, bf16[8,1024,2,64]{1,3,2,0...) while((s32[]{:T(128)}, f32[256,2,2]{0,2,1:T(2,128)S(1)}, ...), condition=%wide.region_21.22_spmd, body=%wide.region_18.21_spmd.sunk | while | flops 276957184 | bytes 13828197 | solution.py:125
  334.7 1.8 fusion.172
  369.4 4.6 all-to-all-start
  374.0 4.7 all-to-all-done
  378.8 3.2 multiply_reduce_fusion
  384.2 3.3 reshape.304
  387.5 102.3 %all_to_all.29 = bf16[64,3,2048]{2,1,0:T(4,128)(2,1)} all-to-all(bf16[64,3,2048]{2,1,0:T(4,128)(2,1)} %reshape.304), channel_id=1, replica_groups=mesh['sp'=64,'tp'=4] {'sp'}, dimensions={0} | all-to-all | bytes 1572864 | tf_op jit(solution)/shard_map/all_to_all | solution.py:32
  489.9 3.2 reshape.305
  493.1 37.1 %all-gather.5.cloned.1.call-done = bf16[768,2048]{1,0:T(8,128)(2,1)} async-done(((bf16[192,2048]{1,0:T(8,128)(2,1)}), bf16[768,2048]{1,0:T(8,128)(2,1)}) %all-gather.5.cloned.1.call-update) | async-done | bytes 3145744 | tf_op jit(solution)/shard_map/all_gather | solution.py:181
  530.2 6.9 %fusion.61 = f32[768,768]{1,0:T(8,128)} fusion(bf16[768,2048]{1,0:T(8,128)(2,1)} %all-gather.5.cloned.1.call-done, bf16[1,2048,768]{2,1,0:T(8,128)(2,1)} %param.30), kind=kOutput, calls=%fused_computation.61 | convolution fusion | flops 2415919104 | bytes 8650752 | tf_op jit(solution)/shard_map/dot_general | solution.py:183
  537.2 11.0 %convolution_convert_fusion = bf16[768,2048]{1,0:T(8,128)(2,1)} fusion(bf16[1,768,2048]{2,1,0:T(8,128)(2,1)S(1)} %copy-done, f32[768,768]{1,0:T(8,128)} %fusion.61, bf16[768,2048]{1,0:T(8,128)(2,1)} %all-gather.5.cloned.1.call-done, bf16[1,2048,768]{2,1,0:T(8,128)(2,1)} %param.29), kind=kOutput, calls=%fused_computation.59 | convolution fusion | flops 4836950016 | bytes 14942208 | tf_op jit(solution)/shard_map/dot_general | solution.py:186
  548.2 41.3 %reduce-scatter.2.cloned.1.call-done = bf16[192,2048]{1,0:T(8,128)(2,1)} async-done(((bf16[768,2048]{1,0:T(8,128)(2,1)}), bf16[192,2048]{1,0:T(8,128)(2,1)}) %reduce-scatter.2.cloned.1.call-update) | async-done | bytes 786448 | tf_op jit(solution)/shard_map/reduce_scatter | solution.py:185
  589.5 3.3 reshape.306
  592.8 38.9 %all_to_all.30 = bf16[64,3,2048]{2,1,0:T(4,128)(2,1)} all-to-all(bf16[64,3,2048]{2,1,0:T(4,128)(2,1)} %reshape.306), channel_id=1, replica_groups=mesh['sp'=64,'tp'=4] {'sp'}, dimensions={0} | all-to-all | bytes 1572864 | tf_op jit(solution)/shard_map/all_to_all | solution.py:196
  631.7 3.2 reshape.322
  (223 shorter events, 106.6 us)
Async XLA Ops:
  6.5 530.6 %copy-start = (bf16[1,768,2048]{2,1,0:T(8,128)(2,1)S(1)}, bf16[1,768,2048]{2,1,0:T(8,128)(2,1)}, u32[]{:S(2)}) copy-start(bf16[1,768,2048]{2,1,0:T(8,128)(2,1)} %param.31) | copy-start | bytes 9437188
  6.5 6.5 %copy-start.12 = (bf16[256,128]{1,0:T(8,128)(2,1)S(1)}, bf16[256,128]{1,0:T(8,128)(2,1)}, u32[]{:S(2)}) copy-start(bf16[256,128]{1,0:T(8,128)(2,1)} %param.22) | copy-start | bytes 196612
  6.5 7.9 %copy-start.24 = (f32[64]{0:T(128)S(1)}, f32[64]{0:T(128)}, u32[]{:S(2)}) copy-start(f32[64]{0:T(128)} %param.23) | copy-start | bytes 772
  6.5 12.2 %copy-start.22 = (s32[64,2]{0,1:T(2,128)S(1)}, s32[64,2]{0,1:T(2,128)}, u32[]{:S(2)}) copy-start(s32[64,2]{0,1:T(2,128)} %param.27) | copy-start | bytes 1540
  6.5 372.3 %all-gather.3.cloned.1.call-start = ((), (), s32[]{:S(2)}) async-start(), calls=%async_computation.4 | async-start | bytes 5242880 | tf_op jit(solution)/shard_map/all_gather | solution.py:87
  8.8 0.6 copy-start.17
  8.8 0.6 copy-start.18
  9.6 14.4 %copy-start.14 = (bf16[256,128]{0,1:T(8,128)(2,1)}, bf16[256,128]{0,1:T(8,128)(2,1)S(1)}, u32[]{:S(2)}) copy-start(bf16[256,128]{0,1:T(8,128)(2,1)S(1)} %convert_element_type.105) | copy-start | bytes 196612
  9.6 14.4 %collective-permute-start = (bf16[256,128]{0,1:T(8,128)(2,1)S(1)}, bf16[256,128]{0,1:T(8,128)(2,1)S(1)}, u32[]{:S(2)}, u32[]{:S(2)}) collective-permute-start(bf16[256,128]{0,1:T(8,128)(2,1)S(1)} %convert_element_type.105), channel_id=1, source_target_pairs={{0,4},{4,0},{8,12},{12,8},{16,20},{20,16},{24,28},{28,24},{32,36},... | collective-permute-start | bytes 196616 | tf_op jit(solution)/shard_map/ppermute | solution.py:16
  10.4 16.8 %collective-permute-start.3 = (bf16[256,128]{1,0:T(8,128)(2,1)}, bf16[256,128]{1,0:T(8,128)(2,1)}, u32[]{:S(2)}, u32[]{:S(2)}) collective-permute-start(bf16[256,128]{1,0:T(8,128)(2,1)} %param.22), channel_id=1, source_target_pairs={{0,4},{4,0},{8,12},{12,8},{16,20},{20,16},{24,28},{28,24},{32,36},... | collective-permute-start | bytes 196616 | tf_op jit(solution)/shard_map/ppermute | solution.py:16
  24.0 3.2 copy-start.10
  24.7 8.9 %collective-permute-start.1 = (bf16[512,128]{0,1:T(8,128)(2,1)}, bf16[512,128]{0,1:T(8,128)(2,1)S(1)}, u32[]{:S(2)}, u32[]{:S(2)}) collective-permute-start(bf16[512,128]{0,1:T(8,128)(2,1)} %pad_maximum_fusion.5), channel_id=1, source_target_pairs={{0,8},{4,12},{8,0},{12,4},{16,24},{20,28},{24,16},{28,20},{32,40},... | collective-permute-start | bytes 393224 | tf_op jit(solution)/shard_map/ppermute | solution.py:16
  28.7 9.2 %collective-permute-start.4 = (bf16[512,128]{1,0:T(8,128)(2,1)}, bf16[512,128]{1,0:T(8,128)(2,1)S(1)}, u32[]{:S(2)}, u32[]{:S(2)}) collective-permute-start(bf16[512,128]{1,0:T(8,128)(2,1)} %pad_maximum_fusion.6), channel_id=1, source_target_pairs={{0,8},{4,12},{8,0},{12,4},{16,24},{20,28},{24,16},{28,20},{32,40},... | collective-permute-start | bytes 393224 | tf_op jit(solution)/shard_map/ppermute | solution.py:16
  33.6 4.4 copy-start.6
  35.2 11.6 %collective-permute-start.2 = (bf16[1024,128]{0,1:T(8,128)(2,1)}, bf16[1024,128]{0,1:T(8,128)(2,1)}, u32[]{:S(2)}, u32[]{:S(2)}) collective-permute-start(bf16[1024,128]{0,1:T(8,128)(2,1)} %pad_maximum_fusion.2), channel_id=1, source_target_pairs={{0,16},{4,20},{8,24},{12,28},{16,0},{20,4},{24,8},{28,12},{32,48},... | collective-permute-start | bytes 786440 | tf_op jit(solution)/shard_map/ppermute | solution.py:16
  38.0 0.7 copy-start.8
  40.2 13.1 %collective-permute-start.5 = (bf16[1024,128]{1,0:T(8,128)(2,1)}, bf16[1024,128]{1,0:T(8,128)(2,1)S(1)}, u32[]{:S(2)}, u32[]{:S(2)}) collective-permute-start(bf16[1024,128]{1,0:T(8,128)(2,1)} %pad_maximum_fusion.3), channel_id=1, source_target_pairs={{0,16},{4,20},{8,24},{12,28},{16,0},{20,4},{24,8},{28,12},{32,48},... | collective-permute-start | bytes 786440 | tf_op jit(solution)/shard_map/ppermute | solution.py:16
  45.4 3.3 copy-start.7
  45.4 3.3 copy-start.11
  45.4 3.3 copy-start.15
  46.9 6.0 copy-start.16
  48.7 6.7 %copy-start.1 = (f32[2,1024,256,2]{2,1,3,0:T(8,128)}, f32[2,1024,256,2]{2,1,3,0:T(8,128)S(1)}, u32[]{:S(2)}) copy-start(f32[2,1024,256,2]{2,1,3,0:T(8,128)S(1)} %get-tuple-element.368) | copy-start | bytes 12582916
  48.7 4.7 copy-start.9
  48.7 4.7 copy-start.13
  50.9 13.6 %collective-permute-start.6 = (bf16[2048,128]{0,1:T(8,128)(2,1)}, bf16[2048,128]{0,1:T(8,128)(2,1)}, u32[]{:S(2)}, u32[]{:S(2)}) collective-permute-start(bf16[2048,128]{0,1:T(8,128)(2,1)} %pad_maximum_fusion), channel_id=1, source_target_pairs={{0,32},{4,36},{8,40},{12,44},{16,48},{20,52},{24,56},{28,60},{32,0... | collective-permute-start | bytes 1572872 | tf_op jit(solution)/shard_map/ppermute | solution.py:16
  53.3 2.8 copy-start.3
  53.3 2.9 copy-start.2
  55.2 19.4 %collective-permute-start.7 = (bf16[2048,128]{1,0:T(8,128)(2,1)}, bf16[2048,128]{1,0:T(8,128)(2,1)}, u32[]{:S(2)}, u32[]{:S(2)}) collective-permute-start(bf16[2048,128]{1,0:T(8,128)(2,1)} %pad_maximum_fusion.1), channel_id=1, source_target_pairs={{0,32},{4,36},{8,40},{12,44},{16,48},{20,52},{24,56},{28,60},{32,0... | collective-permute-start | bytes 1572872 | tf_op jit(solution)/shard_map/ppermute | solution.py:16
  55.4 1.1 copy-start.19
  55.4 1.4 copy-start.20
  83.4 70.8 %collective-permute-start.8 = (bf16[4096,128]{0,1:T(8,128)(2,1)}, bf16[4096,128]{0,1:T(8,128)(2,1)}, u32[]{:S(2)}, u32[]{:S(2)}) collective-permute-start(bf16[4096,128]{0,1:T(8,128)(2,1)} %get-tuple-element.340), channel_id=1, source_target_pairs={{0,64},{4,68},{8,72},{12,76},{16,80},{20,84},{24,88},{28,92},{32,9... | collective-permute-start | bytes 3145736 | tf_op jit(solution)/shard_map/ppermute | solution.py:16
  88.4 88.3 %collective-permute-start.9 = (bf16[4096,128]{1,0:T(8,128)(2,1)}, bf16[4096,128]{1,0:T(8,128)(2,1)}, u32[]{:S(2)}, u32[]{:S(2)}) collective-permute-start(bf16[4096,128]{1,0:T(8,128)(2,1)} %get-tuple-element.338), channel_id=1, source_target_pairs={{0,64},{4,68},{8,72},{12,76},{16,80},{20,84},{24,88},{28,92},{32,9... | collective-permute-start | bytes 3145736 | tf_op jit(solution)/shard_map/ppermute | solution.py:16
  90.1 1.0 copy-start.4
  93.8 1.0 copy-start.4
  189.9 62.3 %collective-permute-start.10 = (bf16[8192,128]{0,1:T(8,128)(2,1)}, bf16[8192,128]{0,1:T(8,128)(2,1)}, u32[]{:S(2)}, u32[]{:S(2)}) collective-permute-start(bf16[8192,128]{0,1:T(8,128)(2,1)} %constant_dynamic-update-slice_fusion.10), channel_id=1, source_target_pairs={{0,128},{4,132},{8,136},{12,140},{16,144},{20,148},{24,152},{28,15... | collective-permute-start | bytes 6291464 | tf_op jit(solution)/shard_map/ppermute | solution.py:16
  196.0 117.3 %collective-permute-start.11 = (bf16[8192,128]{1,0:T(8,128)(2,1)}, bf16[8192,128]{1,0:T(8,128)(2,1)}, u32[]{:S(2)}, u32[]{:S(2)}) collective-permute-start(bf16[8192,128]{1,0:T(8,128)(2,1)} %constant_dynamic-update-slice_fusion.16), channel_id=1, source_target_pairs={{0,128},{4,132},{8,136},{12,140},{16,144},{20,148},{24,152},{28,15... | collective-permute-start | bytes 6291464 | tf_op jit(solution)/shard_map/ppermute | solution.py:16
  367.5 15.4 %copy-start.21 = (f32[2048]{0:T(1024)S(1)}, f32[2048]{0:T(1024)}, u32[]{:S(2)}) copy-start(f32[2048]{0:T(1024)} %param.26) | copy-start | bytes 24580
  369.4 9.4 %all-to-all-start = ((bf16[4,64,256]{2,1,0:T(8,128)(2,1)}), bf16[4,64,256]{2,1,0:T(8,128)(2,1)S(1)}, u32[]{:S(2)}, u32[]{:S(2)}) async-start(bf16[4,64,256]{2,1,0:T(8,128)(2,1)} %copy.141), calls=%async_computation | async-start | bytes 262144 | tf_op jit(solution)/shard_map/all_to_all | solution.py:146
  374.0 156.3 %all-gather.5.cloned.1.call-start = ((), (), s32[]{:S(2)}) async-start(), calls=%async_computation.5 | async-start | bytes 3932160 | tf_op jit(solution)/shard_map/all_gather | solution.py:181
  382.0 0.9 copy-start.5
  493.1 96.4 %reduce-scatter.2.cloned.1.call-start = ((), (), s32[]{:S(2)}) async-start(), calls=%async_computation.6 | async-start | bytes 3932160 | tf_op jit(solution)/shard_map/reduce_scatter | solution.py:185
  548.2 86.7 %copy-start.23 = (f32[64,2]{0,1:T(2,128)S(1)}, f32[64,2]{0,1:T(2,128)}, u32[]{:S(2)}) copy-start(f32[64,2]{0,1:T(2,128)} %param.28) | copy-start | bytes 1540
Sparse Core Ops, SparseCore 0:
  10.7 52.9 all-gather.2
  493.2 36.9 all-gather.4
  548.3 41.1 reduce-scatter.1
where the time goes:
time: 657 us; the launch traced here: 645 us
  waiting for transfers between devices  258 us (39%)
  blocking collectives  141 us (21%)
  local copies, waits for them, and re-layouts  98.7 us (15%)
  matrix products  83.4 us (13%)
  other arithmetic  29.4 us (4%)
  starting transfers between devices  20 us (3%)
  between operations  14 us (2%)
    ppermute x12, waiting for transfers between devices, partner(): lax.ppermute(x, axis, [(i, i ^ 1 << distance) for i in range(lax.axis_siz...  175 us
    all_to_all x1, blocking collectives, grouped_exchange(): lax.all_to_all(group, axis, split_axis=split_dim, concat_axis=concat_dim,...  102 us
    reduce_scatter x1, waiting for transfers between devices, expert_work(): lax.psum_scatter(jnp.dot(lax.slice_in_dim(hidden, 0, sources * slot_count...  41.3 us
    all_to_all x1, blocking collectives, expert_work(): return lax.all_to_all(answer, 'sp', split_axis=0, concat_axis=0, tiled=True)  38.9 us
    all_gather x1, waiting for transfers between devices, expert_work(): row_piece = lax.all_gather(flat_rows, 'tp', axis=0, tiled=True)  37.1 us
    dot_general x18, matrix products, one_block(): jnp.einsum('qkgd,skd->qkgs', rotated_queries, key_block, preferred_elemen...  30.8 us
    dot_general x18, matrix products, one_block(): jnp.einsum('qkgs,skd->qkgd', weights.astype(jnp.bfloat16), value_block, p...  28.5 us
    while x6, local copies, waits for them, and re-layouts, absorb(): return lax.scan(one_block, carry, (key_blocks, value_blocks))[0]  27.1 us
  transfers between devices with their start and end apart: 16, of which 8 were waited for; matrix products, arithmetic and copies ran while one was open for 26% of the time, Pallas kernels for 0%

commit v1 on v0

v1 whole, which is shorter than its diff:
```python
import jax
import jax.numpy as jnp
from jax import lax
from jax.experimental import pallas as pl
from jax.experimental.pallas import tpu as pltpu
from jax.sharding import PartitionSpec as P

GRID_W = 64
EPS = 1e-06
THETA = 10000.0
NZ, NX = 8, 4
CHIPS = NZ * NX
CHUNK = 2
HALF = 128


def turn_tables(offset, count, head_size):
    position = offset + jnp.arange(count, dtype=jnp.int32)
    grid_row = (position // GRID_W).astype(jnp.float32)
    column = (position % GRID_W).astype(jnp.float32)
    pair_index = jnp.arange(head_size // 4, dtype=jnp.float32)
    inverse = THETA ** (-4.0 * pair_index / head_size)
    lane = jnp.arange(2 * head_size, dtype=jnp.int32) % head_size
    pair = lane // 2
    wide_inverse = jnp.tile(jnp.repeat(inverse, 2), 4)
    place = jnp.where((pair < head_size // 4)[None, :], grid_row[:, None], column[:, None])
    angles = place * wide_inverse
    sign = jnp.where(lane % 2 == 1, 1.0, -1.0)
    return jnp.cos(angles), jnp.sin(angles) * sign


def normalize_turn(x, gain, cosine, sine):
    lane = lax.broadcasted_iota(jnp.int32, x.shape, 1)
    low = lane < 64
    squares = x * x
    first = jnp.sum(jnp.where(low, squares, 0.0), axis=1, keepdims=True)
    second = jnp.sum(jnp.where(low, 0.0, squares), axis=1, keepdims=True)
    mean = jnp.where(low, first, second) * (1.0 / 64)
    wide = x * lax.rsqrt(mean + EPS) * gain
    other = jnp.where(lane % 2 == 1, pltpu.roll(wide, 1, 1), pltpu.roll(wide, 127, 1))
    return wide * cosine + other * sine


def attention_kernel(
    q_ref, k_ref, v_ref, qg_ref, kg_ref, cos_ref, sin_ref, o_ref,
    kv, qz, top, total, acc, send_sem, recv_sem,
):
    me = lax.axis_index("sp")
    core = me % 2
    x = (me // 2) % NX
    z = me // (2 * NX)

    def slot_of(zz, xx, cc):
        return ((zz % NZ) * NX + xx % NX) * 2 + cc

    partner = slot_of(z, x, 1 - core)
    x_up, x_down = slot_of(z, x + 1, core), slot_of(z, x + NX - 1, core)
    z_up, z_down = slot_of(z + 1, x, core), slot_of(z + NZ - 1, x, core)

    barrier = pltpu.get_barrier_semaphore()
    for there in (partner, x_up, x_down, z_up, z_down):
        pl.semaphore_signal(
            barrier, inc=1, device_id={"sp": there}, device_id_type=pl.DeviceIdType.MESH
        )

    cosine, sine = cos_ref[...], sin_ref[...]
    turned = normalize_turn(k_ref[...].astype(jnp.float32), kg_ref[...], cosine, sine).astype(
        jnp.bfloat16
    )
    values_t = v_ref[...].astype(jnp.float32).T.astype(jnp.bfloat16)
    for i in range(2):
        kv[me, i, 0:HALF, :] = turned[i * HALF : (i + 1) * HALF]
        kv[me, i, HALF : 2 * HALF, :] = values_t[:, i * HALF : (i + 1) * HALF]
    pl.semaphore_wait(barrier, 5)

    def copy(slot, half, there):
        return pltpu.make_async_remote_copy(
            src_ref=kv.at[slot, half],
            dst_ref=kv.at[slot, half],
            send_sem=send_sem.at[half],
            recv_sem=recv_sem.at[slot, half],
            device_id={"sp": there},
            device_id_type=pl.DeviceIdType.MESH,
        )

    def arrived(slot, half):
        copy(slot, half, partner).wait_recv()

    def steps(n):
        kz, kx = n // NX, n % NX
        zz = z + NZ + (1 - 2 * (kz % 2)) * ((kz + 1) // 2)
        xx = x + NX + (1 - 2 * (kx % 2)) * ((kx + 1) // 2)
        return kz, kx, zz, xx

    def move(n):
        kz, kx, zz, xx = steps(n)
        slot = slot_of(zz, xx, core)

        @pl.when(n > 0)
        def _():
            arrived(slot, 0)
            arrived(slot, 1)

        z_plus = (kz == 0) | ((kz % 2 == 1) & (kz < 5)) | ((kz == 5) & (core == 0))
        z_minus = (kz == 0) | ((kz % 2 == 0) & (kz < 6)) | ((kz == 6) & (core == 1))
        x_plus = (kx == 0) | ((kx == 1) & (core == 0))
        x_minus = (kx == 0) | ((kx == 2) & (core == 1))

        @pl.when((kx == 0) & z_plus)
        def _():
            copy(slot, 1, z_up).start()

        @pl.when((kx == 0) & z_minus)
        def _():
            copy(slot, 1, z_down).start()

        @pl.when((kz == 0) & x_plus)
        def _():
            copy(slot, 0, x_up).start()

        @pl.when((kz == 0) & x_minus)
        def _():
            copy(slot, 0, x_down).start()

        @pl.when(z_plus)
        def _():
            copy(slot, 0, z_up).start()

        @pl.when(z_minus)
        def _():
            copy(slot, 0, z_down).start()

        @pl.when(x_plus)
        def _():
            copy(slot, 1, x_up).start()

        @pl.when(x_minus)
        def _():
            copy(slot, 1, x_down).start()

        copy(slot, 0, partner).start()
        copy(slot, 1, partner).start()

    move(0)

    for h in range(2):
        part = q_ref[:, h * 128 : (h + 1) * 128].astype(jnp.float32)
        rows = normalize_turn(part, qg_ref[...], cosine, sine).astype(jnp.bfloat16)
        across = (rows.astype(jnp.float32).T * 0.125).astype(jnp.bfloat16)
        qz[h, h * 64 : (h + 1) * 64, 0:256] = across[0:64]
        qz[h, h * 64 : (h + 1) * 64, 256:512] = across[64:128]
        qz[h, (1 - h) * 64 : (2 - h) * 64, :] = jnp.zeros((64, 512), jnp.bfloat16)
    top[...] = jnp.full(top.shape, -1e30, jnp.float32)
    total[...] = jnp.zeros(total.shape, jnp.float32)
    acc[...] = jnp.zeros(acc.shape, jnp.float32)

    for n in range(1, CHUNK):
        move(n)

    def body(step, carry):
        @pl.when(step + 1 < CHIPS // CHUNK)
        def _():
            for i in range(CHUNK):
                move((step + 1) * CHUNK + i)

        blocks = []
        for i in range(CHUNK):
            _, _, zz, xx = steps(step * CHUNK + i)
            theirs = slot_of(zz, xx, 1 - core)
            arrived(theirs, 0)
            arrived(theirs, 1)
            first = slot_of(zz, xx, 0)
            blocks += [kv.at[first + c, j] for c in range(2) for j in range(2)]
        keys = jnp.concatenate([b[0:HALF, :] for b in blocks], axis=0)
        scores = [jnp.dot(keys, qz[h], preferred_element_type=jnp.float32) for h in range(2)]
        for h in range(2):
            old = top[h]
            new = jnp.maximum(old, jnp.max(scores[h], axis=0, keepdims=True))
            weights = jnp.exp(scores[h] - new)
            shrink = jnp.exp(old - new)
            top[h] = new
            total[h] = total[h] * shrink + jnp.sum(weights, axis=0, keepdims=True)
            vt = jnp.concatenate(
                [b[HALF + h * 64 : HALF + (h + 1) * 64, :] for b in blocks], axis=1
            )
            acc[h] = acc[h] * shrink + jnp.dot(
                vt, weights.astype(jnp.bfloat16), preferred_element_type=jnp.float32
            )
        return carry

    lax.fori_loop(0, CHIPS // CHUNK, body, 0)
    parts = []
    for h in range(2):
        mixed = acc[h] / total[h]
        parts += [mixed[:, 0:256], mixed[:, 256:512]]
    o_ref[...] = jnp.concatenate(parts, axis=0).T.astype(jnp.bfloat16)
    for half in range(2):
        everything = kv.at[pl.ds(0, 63), half]
        pltpu.make_async_copy(everything, everything, send_sem.at[half]).wait()


def attention(queries, keys, values, query_gain, key_gain, cosine, sine):
    vmem = pl.BlockSpec(memory_space=pltpu.VMEM)
    return pl.pallas_call(
        attention_kernel,
        out_shape=jax.ShapeDtypeStruct((256, 256), jnp.bfloat16),
        in_specs=[vmem] * 7,
        out_specs=vmem,
        scratch_shapes=[
            pltpu.VMEM((2 * CHIPS, 2, 2 * HALF, 128), jnp.bfloat16),
            pltpu.VMEM((2, 128, 512), jnp.bfloat16),
            pltpu.VMEM((2, 1, 512), jnp.float32),
            pltpu.VMEM((2, 1, 512), jnp.float32),
            pltpu.VMEM((2, 64, 512), jnp.float32),
            pltpu.SemaphoreType.DMA((2,)),
            pltpu.SemaphoreType.DMA((2 * CHIPS, 2)),
        ],
        compiler_params=pltpu.CompilerParams(
            collective_id=0, has_side_effects=True, vmem_limit_bytes=40 * 2**20
        ),
        cost_estimate=pl.CostEstimate(
            flops=8 * 10**9, bytes_accessed=2**20, transcendentals=2**24
        ),
        name="attention",
    )(queries, keys, values, query_gain, key_gain, cosine, sine)


def local(
    stream_in, queries, keys, values, query_gain, key_gain, out_rows, norm_gain,
    route_ids, route_weights, gate_weight, up_weight, down_weight,
):
    head_size = query_gain.shape[0]
    seq_rows = queries.shape[0]
    whole_out = lax.all_gather(out_rows, "tp", axis=0, tiled=True)
    cosine, sine = turn_tables(lax.axis_index("sp") * seq_rows, seq_rows, head_size)
    twice = lambda g: jnp.tile(g, 2)[None, :]
    attended = attention(
        queries, keys, values, twice(query_gain), twice(key_gain), cosine, sine
    )
    token_heads = lax.all_to_all(attended, "tp", split_axis=0, concat_axis=1, tiled=True)
    projected = jnp.dot(token_heads, whole_out, preferred_element_type=jnp.float32)
    stream = (stream_in.astype(jnp.float32) + projected).astype(jnp.bfloat16)
    stream_wide = stream.astype(jnp.float32)
    normed = (
        stream_wide
        * lax.rsqrt(jnp.mean(stream_wide * stream_wide, axis=1, keepdims=True) + EPS)
        * norm_gain
    ).astype(jnp.bfloat16)
    tokens = stream.shape[0]
    model_width = stream.shape[1]
    top_count = route_ids.shape[1]
    experts = lax.axis_size("sp")
    routed = tokens * top_count
    capacity = 3
    flat_ids = route_ids.reshape(routed)
    member = (flat_ids[:, None] == jnp.arange(experts, dtype=jnp.int32)[None, :]).astype(jnp.int32)
    earlier = jnp.cumsum(member, axis=0) - member
    slot_rank = jnp.sum(earlier * member, axis=1)
    target = flat_ids * capacity + slot_rank
    placed = (target[:, None] == jnp.arange(experts * capacity, dtype=jnp.int32)[None, :]).astype(
        jnp.bfloat16
    )
    placed = placed.reshape(tokens, top_count, experts * capacity)
    outgoing = jnp.einsum("tks,td->sd", placed, normed, preferred_element_type=jnp.float32).astype(
        jnp.bfloat16
    )
    outgoing = outgoing.reshape(experts, capacity, model_width)
    arrived = lax.all_to_all(outgoing, "sp", split_axis=0, concat_axis=0, tiled=True)
    flat_rows = arrived.reshape(experts * capacity, model_width)
    row_piece = lax.all_gather(flat_rows, "tp", axis=0, tiled=True)
    gate_value = jnp.dot(row_piece, gate_weight[0], preferred_element_type=jnp.float32)
    up_value = jnp.dot(row_piece, up_weight[0], preferred_element_type=jnp.float32)
    hidden = (jax.nn.silu(gate_value) * up_value).astype(jnp.bfloat16)
    summed = lax.psum_scatter(
        jnp.dot(hidden, down_weight[0], preferred_element_type=jnp.float32).astype(jnp.bfloat16),
        "tp",
        scatter_dimension=0,
        tiled=True,
    )
    answer = summed.reshape(experts, capacity, model_width)
    returned = lax.all_to_all(answer, "sp", split_axis=0, concat_axis=0, tiled=True)
    expert_back = returned.reshape(experts * capacity, model_width)
    picked = jnp.einsum("tks,sd->tkd", placed, expert_back, preferred_element_type=jnp.float32)
    mixed_out = stream_wide + jnp.sum(route_weights[:, :, None] * picked, axis=1)
    return mixed_out.astype(jnp.bfloat16)


def solution(mesh):
    return jax.shard_map(
        local,
        mesh=mesh,
        in_specs=(
            P(("sp", "tp"), None),
            P("sp", "tp"),
            P("sp", "tp"),
            P("sp", "tp"),
            P(),
            P(),
            P("tp", None),
            P(),
            P(("sp", "tp"), None),
            P(("sp", "tp"), None),
            P("sp", None, "tp"),
            P("sp", None, "tp"),
            P("sp", "tp", None),
        ),
        out_specs=P(("sp", "tp"), None),
        check_vma=False,
    )
```

time: 657 us -> 312 us (0.47); the launches traced: 645 us -> 310 us
  waiting for transfers between devices: 258 us -> 83.1 us
  Pallas kernels: 0 us -> 83.1 us
  local copies, waits for them, and re-layouts: 98.7 us -> 18.8 us
  blocking collectives: 141 us -> 80.1 us
  matrix products: 83.4 us -> 23.9 us
  other arithmetic: 29.4 us -> 2.93 us
  starting transfers between devices: 20 us -> 4.82 us
    ppermute x12 -> x0, waiting for transfers between devices: 175 us -> none  [partner(): lax.ppermute(x, axis, [(i, i ^ 1 << distance) for i in range(lax.axis_siz...]
    pallas_call x0 -> x1, Pallas kernels: none -> 83.1 us  [attention(): pl.pallas_call(attention_kernel, out_shape=jax.ShapeDtypeStruct((256, 256...]
    all_to_all x2, blocking collectives: 141 us -> 80.1 us  [the longest x1 41.2 us: local(): lax.all_to_all(outgoing, 'sp', split_axis=0, concat_axis=0, tiled=True)]
    dot_general x38 -> x2, matrix products: 77.3 us -> 17.9 us  [the longest x1 11 us: local(): jnp.dot(hidden, down_weight[0], preferred_element_type=jnp.float32)]
    while x24 -> x0, local copies, waits for them, and re-layouts: 27.7 us -> none  [the longest x6 27.1 us: absorb(): return lax.scan(one_block, carry, (key_blocks, value_blocks))[0]]
    reshape x9 -> x2, local copies, waits for them, and re-layouts: 28.6 us -> 6.45 us  [the longest x1 3.28 us: local(): answer = summed.reshape(experts, capacity, model_width)]
    unnamed x63 -> x17, local copies, waits for them, and re-layouts: 22.5 us -> 3.54 us
    ppermute x12 -> x0, starting transfers between devices: 15.4 us -> none  [partner(): lax.ppermute(x, axis, [(i, i ^ 1 << distance) for i in range(lax.axis_siz...]
  transfers between devices with their start and end apart: 16 -> 4, of which waited for: 8 -> 3; matrix products, arithmetic and copies ran while one was open for 26% -> 1% of each run, Pallas kernels for 0% -> 27%
where the time goes in v1:
time: 312 us; the launch traced here: 310 us
  waiting for transfers between devices  83.1 us (27%)
  Pallas kernels  83.1 us (27%)
  blocking collectives  80.1 us (26%)
  matrix products  23.9 us (8%)
  local copies, waits for them, and re-layouts  18.8 us (6%)
  between operations  13.2 us (4%)
  starting transfers between devices  4.82 us (2%)
    pallas_call x1, Pallas kernels, attention(): pl.pallas_call(attention_kernel, out_shape=jax.ShapeDtypeStruct((256, 256...  83.1 us
    reduce_scatter x1, waiting for transfers between devices, local(): lax.psum_scatter(jnp.dot(hidden, down_weight[0], preferred_element_type=j...  41.3 us
    all_to_all x1, blocking collectives, local(): lax.all_to_all(outgoing, 'sp', split_axis=0, concat_axis=0, tiled=True)  41.2 us
    all_to_all x1, blocking collectives, local(): lax.all_to_all(answer, 'sp', split_axis=0, concat_axis=0, tiled=True)  38.9 us
    all_gather x1, waiting for transfers between devices, local(): row_piece = lax.all_gather(flat_rows, 'tp', axis=0, tiled=True)  36.9 us
    dot_general x1, matrix products, local(): jnp.dot(hidden, down_weight[0], preferred_element_type=jnp.float32)  11 us
    dot_general x1, matrix products, local(): jnp.dot(row_piece, up_weight[0], preferred_element_type=jnp.float32)  6.87 us
  transfers between devices with their start and end apart: 4, of which 3 were waited for; matrix products, arithmetic and copies ran while one was open for 1% of the time, Pallas kernels for 27%

profile of v1, /device:TPU:33, one launch (start us, length us, event | category | flops | bytes accessed | tf_op | source)
XLA Modules:
  0.0 310.0 jit_solution(18245066075267719053)
XLA Ops:
  6.5 0.0 copy-start
  6.5 0.7 all-gather.3.cloned.1.call-update
  7.3 0.9 tile.8
  8.1 0.1 broadcast_in_dim_tile.7.qg_ref
  8.2 0.7 tile.9
  8.9 0.1 broadcast_in_dim_tile.8.kg_ref
  9.0 0.1 broadcast_in_dim.48
  9.0 0.1 tile.10
  9.2 0.1 mul.70
  9.3 0.5 sine_multiply_fusion
  9.8 0.0 copy-start.1
  9.8 0.9 copy-done.1
  10.7 0.8 copy-done.2
  11.6 0.8 copy-done.3
  12.4 83.1 %attention.1 = bf16[256,256]{1,0:T(8,128)(2,1)} custom-call(bf16[256,256]{1,0:T(8,128)(2,1)S(1)} %copy-done.1, bf16[256,128]{1,0:T(8,128)(2,1)S(1)} %copy-done.2, bf16[256,128]{1,0:T(8,128)(2,1)S(1)} %copy-done.3, f32[1,128]{1,0:T(1,128)S(1)} %broadcast_in_dim_tile.7.qg_ref, f32[1,128]{1,0:T(1,128)S(1)} %broadcast_in_dim_tile.8.kg_ref, ...), custom_call_target="tpu_custom_call" | custom-call | flops 8000000000 | bytes 1048576 | tf_op jit(solution)/shard_map/attention/pallas_call | solution.py:204
  95.5 0.0 copy-start.5
  95.5 4.6 %all-to-all-start = ((bf16[4,64,256]{2,1,0:T(8,128)(2,1)}), bf16[4,64,256]{2,1,0:T(8,128)(2,1)S(1)}, u32[]{:S(2)}, u32[]{:S(2)}) async-start(bf16[4,64,256]{2,1,0:T(8,128)(2,1)} %bitcast), calls=%async_computation | async-start | bytes 262144 | tf_op jit(solution)/shard_map/all_to_all | solution.py:240
  100.1 0.1 copy.35
  100.2 0.1 eq.65
  100.3 0.1 fusion.19
  100.4 0.2 reduce_window_sum.11
  100.6 0.2 select_reduce_fusion
  100.8 0.1 reduce_sum.39
  100.9 0.1 copy.36
  101.0 0.1 convert_reduce_fusion
  101.1 4.1 %all-to-all-done = bf16[4,64,256]{2,1,0:T(8,128)(2,1)S(1)} async-done(((bf16[4,64,256]{2,1,0:T(8,128)(2,1)}), bf16[4,64,256]{2,1,0:T(8,128)(2,1)S(1)}, u32[]{:S(2)}, u32[]{:S(2)}) %all-to-all-start) | async-done | bytes 131104 | tf_op jit(solution)/shard_map/all_to_all | solution.py:240
  105.3 0.0 all-gather.3.cloned.1.call-done
  105.3 3.2 %multiply_reduce_fusion = (f32[64]{0:T(128)S(1)}, f32[64,2048]{1,0:T(8,128)S(1)}) fusion(bf16[64,1024]{1,0:T(8,128)(2,1)S(1)} %bitcast.27, bf16[1024,2048]{1,0:T(8,128)(2,1)} %all-gather.3.cloned.1.call-done, bf16[64,2048]{1,0:T(8,128)(2,1)} %param.13), kind=kOutput, calls=%fused_computation.15 | convolution fusion | flops 269221824 | bytes 5112064 | tf_op jit(solution)/shard_map/dot_general | solution.py:241
  108.5 0.8 copy-done.4
  109.3 1.3 convolution_convert_fusion.1
  110.7 3.3 %reshape.144 = bf16[64,3,2048]{2,1,0:T(4,128)(2,1)} reshape(bf16[192,2048]{1,0:T(8,128)(2,1)} %convolution_convert_fusion.1) | data formatting | bytes 1572864 | tf_op jit(solution)/shard_map/reshape | solution.py:267
  114.0 41.2 %all_to_all.29 = bf16[64,3,2048]{2,1,0:T(4,128)(2,1)} all-to-all(bf16[64,3,2048]{2,1,0:T(4,128)(2,1)} %reshape.144), channel_id=1, replica_groups=mesh['sp'=64,'tp'=4] {'sp'}, dimensions={0} | all-to-all | bytes 1572864 | tf_op jit(solution)/shard_map/all_to_all | solution.py:268
  155.2 3.2 %reshape.145 = bf16[192,2048]{1,0:T(8,128)(2,1)} reshape(bf16[64,3,2048]{2,1,0:T(4,128)(2,1)} %all_to_all.29) | data formatting | bytes 1572864 | tf_op jit(solution)/shard_map/reshape | solution.py:269
  158.3 0.0 all-gather.5.cloned.1.call-update
  158.4 0.2 reduce-scatter.2.cloned.1.call-start
  158.6 36.9 %all-gather.5.cloned.1.call-done = bf16[768,2048]{1,0:T(8,128)(2,1)} async-done(((bf16[192,2048]{1,0:T(8,128)(2,1)}), bf16[768,2048]{1,0:T(8,128)(2,1)}) %all-gather.5.cloned.1.call-update) | async-done | bytes 3145744 | tf_op jit(solution)/shard_map/all_gather | solution.py:270
  195.5 6.9 %fusion.1 = f32[768,768]{1,0:T(8,128)} fusion(bf16[768,2048]{1,0:T(8,128)(2,1)} %all-gather.5.cloned.1.call-done, bf16[1,2048,768]{2,1,0:T(8,128)(2,1)} %param.24), kind=kOutput, calls=%fused_computation.2 | convolution fusion | flops 2415919104 | bytes 8650752 | tf_op jit(solution)/shard_map/dot_general | solution.py:272
  202.4 0.0 copy-done
  202.4 11.0 %convolution_convert_fusion = bf16[768,2048]{1,0:T(8,128)(2,1)} fusion(bf16[1,768,2048]{2,1,0:T(8,128)(2,1)S(1)} %copy-done, f32[768,768]{1,0:T(8,128)} %fusion.1, bf16[768,2048]{1,0:T(8,128)(2,1)} %all-gather.5.cloned.1.call-done, bf16[1,2048,768]{2,1,0:T(8,128)(2,1)} %param.23), kind=kOutput, calls=%fused_computation | convolution fusion | flops 4836950016 | bytes 14942208 | tf_op jit(solution)/shard_map/dot_general | solution.py:275
  213.4 0.0 reduce-scatter.2.cloned.1.call-update
  213.4 0.0 copy-start.7
  213.4 41.3 %reduce-scatter.2.cloned.1.call-done = bf16[192,2048]{1,0:T(8,128)(2,1)} async-done(((bf16[768,2048]{1,0:T(8,128)(2,1)}), bf16[192,2048]{1,0:T(8,128)(2,1)}) %reduce-scatter.2.cloned.1.call-update) | async-done | bytes 786448 | tf_op jit(solution)/shard_map/reduce_scatter | solution.py:274
  254.7 3.3 %reshape.146 = bf16[64,3,2048]{2,1,0:T(4,128)(2,1)} reshape(bf16[192,2048]{1,0:T(8,128)(2,1)} %reduce-scatter.2.cloned.1.call-done) | data formatting | bytes 1572864 | tf_op jit(solution)/shard_map/reshape | solution.py:280
  258.0 38.9 %all_to_all.30 = bf16[64,3,2048]{2,1,0:T(4,128)(2,1)} all-to-all(bf16[64,3,2048]{2,1,0:T(4,128)(2,1)} %reshape.146), channel_id=1, replica_groups=mesh['sp'=64,'tp'=4] {'sp'}, dimensions={0} | all-to-all | bytes 1572864 | tf_op jit(solution)/shard_map/all_to_all | solution.py:281
  296.9 3.2 %reshape.148 = bf16[192,2048,1]{1,0,2:T(8,128)(2,1)} reshape(bf16[64,3,2048]{2,1,0:T(4,128)(2,1)} %all_to_all.30) | data formatting | bytes 1572864 | tf_op jit(solution)/shard_map/reshape | solution.py:282
  300.1 0.0 copy-done.7
  300.1 1.5 fusion.9
  301.7 1.8 add_convert_fusion
  (16 shorter events, 0.1 us)
Async XLA Ops:
  6.5 195.9 %copy-start = (bf16[1,768,2048]{2,1,0:T(8,128)(2,1)S(1)}, bf16[1,768,2048]{2,1,0:T(8,128)(2,1)}, u32[]{:S(2)}) copy-start(bf16[1,768,2048]{2,1,0:T(8,128)(2,1)} %param.25) | copy-start | bytes 9437188
  6.5 98.7 %all-gather.3.cloned.1.call-start = ((), (), s32[]{:S(2)}) async-start(), calls=%async_computation.4 | async-start | bytes 5242880 | tf_op jit(solution)/shard_map/all_gather | solution.py:234
  9.8 0.9 copy-start.1
  10.7 0.8 copy-start.2
  11.6 0.8 copy-start.3
  12.4 87.7 %copy-start.6 = (s32[64,2]{0,1:T(2,128)S(1)}, s32[64,2]{0,1:T(2,128)}, u32[]{:S(2)}) copy-start(s32[64,2]{0,1:T(2,128)} %param.21) | copy-start | bytes 1540
  95.5 13.8 %copy-start.5 = (f32[2048]{0:T(1024)S(1)}, f32[2048]{0:T(1024)}, u32[]{:S(2)}) copy-start(f32[2048]{0:T(1024)} %param.20) | copy-start | bytes 24580
  95.5 9.7 %all-to-all-start = ((bf16[4,64,256]{2,1,0:T(8,128)(2,1)}), bf16[4,64,256]{2,1,0:T(8,128)(2,1)S(1)}, u32[]{:S(2)}, u32[]{:S(2)}) async-start(bf16[4,64,256]{2,1,0:T(8,128)(2,1)} %bitcast), calls=%async_computation | async-start | bytes 262144 | tf_op jit(solution)/shard_map/all_to_all | solution.py:240
  100.1 95.4 %all-gather.5.cloned.1.call-start = ((), (), s32[]{:S(2)}) async-start(), calls=%async_computation.5 | async-start | bytes 3932160 | tf_op jit(solution)/shard_map/all_gather | solution.py:270
  108.5 0.9 copy-start.4
  158.4 96.4 %reduce-scatter.2.cloned.1.call-start = ((), (), s32[]{:S(2)}) async-start(), calls=%async_computation.6 | async-start | bytes 3932160 | tf_op jit(solution)/shard_map/reduce_scatter | solution.py:274
  213.4 86.7 %copy-start.7 = (f32[64,2]{0,1:T(2,128)S(1)}, f32[64,2]{0,1:T(2,128)}, u32[]{:S(2)}) copy-start(f32[64,2]{0,1:T(2,128)} %param.22) | copy-start | bytes 1540
Sparse Core Ops, SparseCore 0:
  9.1 53.2 all-gather.2
  158.5 36.9 all-gather.4
  213.5 41.1 reduce-scatter.1

commit v2 on v1

--- a/solution.py
+++ b/solution.py
@@ -8,9 +8,12 @@
 GRID_W = 64
 EPS = 1e-06
 THETA = 10000.0
-NZ, NX = 8, 4
+NZ, NX, NY = 8, 4, 4
 CHIPS = NZ * NX
-CHUNK = 2
+CHUNK = 1
+AHEAD = 3
+WEIGHTS_AT = 16
+SLOTS = 3
 HALF = 128
 
 
@@ -42,13 +45,15 @@
 
 
 def attention_kernel(
-    q_ref, k_ref, v_ref, qg_ref, kg_ref, cos_ref, sin_ref, o_ref,
-    kv, qz, top, total, acc, send_sem, recv_sem,
+    q_ref, k_ref, v_ref, qg_ref, kg_ref, cos_ref, sin_ref, w_ref, t_ref, whole_ref,
+    kv, qz, top, total, acc, own, send_sem, recv_sem, w_sem, t_sem,
 ):
     me = lax.axis_index("sp")
     core = me % 2
     x = (me // 2) % NX
     z = me // (2 * NX)
+    y = lax.axis_index("tp")
+    y_up, y_far, y_down = (y + 1) % NY, (y + 2) % NY, (y + 3) % NY
 
     def slot_of(zz, xx, cc):
         return ((zz % NZ) * NX + xx % NX) * 2 + cc
@@ -61,6 +66,22 @@
     for there in (partner, x_up, x_down, z_up, z_down):
         pl.semaphore_signal(
             barrier, inc=1, device_id={"sp": there}, device_id_type=pl.DeviceIdType.MESH
+        )
+
+    for there in (y_up, y_far, y_down):
+        pl.semaphore_signal(
+            barrier, inc=1, device_id={"tp": there}, device_id_type=pl.DeviceIdType.MESH
+        )
+
+    def share(source, there):
+        part = whole_ref.at[pl.ds(pl.multiple_of(source * 256, 256), 256)]
+        return pltpu.make_async_remote_copy(
+            src_ref=part,
+            dst_ref=part,
+            send_sem=send_sem.at[1],
+            recv_sem=w_sem.at[source],
+            device_id={"tp": there},
+            device_id_type=pl.DeviceIdType.MESH,
         )
 
     cosine, sine = cos_ref[...], sin_ref[...]
@@ -71,23 +92,28 @@
     for i in range(2):
         kv[me, i, 0:HALF, :] = turned[i * HALF : (i + 1) * HALF]
         kv[me, i, HALF : 2 * HALF, :] = values_t[:, i * HALF : (i + 1) * HALF]
-    pl.semaphore_wait(barrier, 5)
-
-    def copy(slot, half, there):
+    whole_ref[pl.ds(pl.multiple_of(y * 256, 256), 256), :] = w_ref[...]
+    pl.semaphore_wait(barrier, 8)
+
+    def copy(slot, there):
         return pltpu.make_async_remote_copy(
-            src_ref=kv.at[slot, half],
-            dst_ref=kv.at[slot, half],
-            send_sem=send_sem.at[half],
-            recv_sem=recv_sem.at[slot, half],
+            src_ref=kv.at[slot],
+            dst_ref=kv.at[slot],
+            send_sem=send_sem.at[0],
+            recv_sem=recv_sem.at[slot],
             device_id={"sp": there},
             device_id_type=pl.DeviceIdType.MESH,
         )
 
-    def arrived(slot, half):
-        copy(slot, half, partner).wait_recv()
+    def arrived(slot):
+        copy(slot, partner).wait_recv()
 
     def steps(n):
-        kz, kx = n // NX, n % NX
+        near = n - NX
+        kz = jnp.where(n < NX, 0, 2 * (near // (2 * NX)) + 1 + near % 2)
+        kz = jnp.where(n < CHIPS - NX, kz, NZ - 1)
+        kx = jnp.where(n < NX, n, (near % (2 * NX)) // 2)
+        kx = jnp.where(n < CHIPS - NX, kx, n % NX)
         zz = z + NZ + (1 - 2 * (kz % 2)) * ((kz + 1) // 2)
         xx = x + NX + (1 - 2 * (kx % 2)) * ((kx + 1) // 2)
         return kz, kx, zz, xx
@@ -98,50 +124,38 @@
 
         @pl.when(n > 0)
         def _():
-            arrived(slot, 0)
-            arrived(slot, 1)
-
-        z_plus = (kz == 0) | ((kz % 2 == 1) & (kz < 5)) | ((kz == 5) & (core == 0))
-        z_minus = (kz == 0) | ((kz % 2 == 0) & (kz < 6)) | ((kz == 6) & (core == 1))
-        x_plus = (kx == 0) | ((kx == 1) & (core == 0))
-        x_minus = (kx == 0) | ((kx == 2) & (core == 1))
-
-        @pl.when((kx == 0) & z_plus)
-        def _():
-            copy(slot, 1, z_up).start()
-
-        @pl.when((kx == 0) & z_minus)
-        def _():
-            copy(slot, 1, z_down).start()
-
-        @pl.when((kz == 0) & x_plus)
-        def _():
-            copy(slot, 0, x_up).start()
-
-        @pl.when((kz == 0) & x_minus)
-        def _():
-            copy(slot, 0, x_down).start()
-
-        @pl.when(z_plus)
-        def _():
-            copy(slot, 0, z_up).start()
-
-        @pl.when(z_minus)
-        def _():
-            copy(slot, 0, z_down).start()
-
-        @pl.when(x_plus)
-        def _():
-            copy(slot, 1, x_up).start()
-
-        @pl.when(x_minus)
-        def _():
-            copy(slot, 1, x_down).start()
-
-        copy(slot, 0, partner).start()
-        copy(slot, 1, partner).start()
+            arrived(slot)
+
+        z_long = jnp.where(core == 0, kx % 2, 0)
+        x_long = jnp.where(core == 0, 1, kz % 2)
+        z_plus = (kz == 0) | ((kz % 2 == 1) & (kz < 5)) | ((kz == 5) & (z_long == 1))
+        z_minus = (kz == 0) | ((kz % 2 == 0) & (kz < 6)) | ((kz == 6) & (z_long == 0))
+        x_plus = (kx == 0) | ((kx == 1) & (x_long == 1))
+        x_minus = (kx == 0) | ((kx == 2) & (x_long == 0))
+        on_z = (core == 0) | (kx == 0)
+        on_x = (core == 1) | (kz == 0)
+
+        @pl.when(on_z & z_plus)
+        def _():
+            copy(slot, z_up).start()
+
+        @pl.when(on_z & z_minus)
+        def _():
+            copy(slot, z_down).start()
+
+        @pl.when(on_x & x_plus)
+        def _():
+            copy(slot, x_up).start()
+
+        @pl.when(on_x & x_minus)
+        def _():
+            copy(slot, x_down).start()
+
+        copy(slot, partner).start()
 
     move(0)
+    share(y, y_up).start()
+    share(y, y_down).start()
 
     for h in range(2):
         part = q_ref[:, h * 128 : (h + 1) * 128].astype(jnp.float32)
@@ -154,21 +168,34 @@
     total[...] = jnp.zeros(total.shape, jnp.float32)
     acc[...] = jnp.zeros(acc.shape, jnp.float32)
 
-    for n in range(1, CHUNK):
+    for n in range(1, CHUNK + AHEAD):
         move(n)
 
     def body(step, carry):
-        @pl.when(step + 1 < CHIPS // CHUNK)
-        def _():
-            for i in range(CHUNK):
-                move((step + 1) * CHUNK + i)
+        for i in range(CHUNK):
+            n = step * CHUNK + CHUNK + AHEAD + i
+
+            @pl.when(n < CHIPS)
+            def _():
+                move(n)
+
+        @pl.when(step == WEIGHTS_AT // CHUNK)
+        def _():
+            share(y_down, y_up).wait_recv()
+            share(y_up, y_down).wait_recv()
+
+            @pl.when(core == 0)
+            def _():
+                share(y_down, y_up).start()
+
+            @pl.when(core == 1)
+            def _():
+                share(y_up, y_down).start()
 
         blocks = []
         for i in range(CHUNK):
             _, _, zz, xx = steps(step * CHUNK + i)
-            theirs = slot_of(zz, xx, 1 - core)
-            arrived(theirs, 0)
-            arrived(theirs, 1)
+            arrived(slot_of(zz, xx, 1 - core))
             first = slot_of(zz, xx, 0)
             blocks += [kv.at[first + c, j] for c in range(2) for j in range(2)]
         keys = jnp.concatenate([b[0:HALF, :] for b in blocks], axis=0)
@@ -193,27 +220,56 @@
     for h in range(2):
         mixed = acc[h] / total[h]
         parts += [mixed[:, 0:256], mixed[:, 256:512]]
-    o_ref[...] = jnp.concatenate(parts, axis=0).T.astype(jnp.bfloat16)
-    for half in range(2):
-        everything = kv.at[pl.ds(0, 63), half]
-        pltpu.make_async_copy(everything, everything, send_sem.at[half]).wait()
-
-
-def attention(queries, keys, values, query_gain, key_gain, cosine, sine):
+    own[...] = jnp.concatenate(parts, axis=0).T.astype(jnp.bfloat16)
+
+    def rows(source, there):
+        columns = pl.ds(pl.multiple_of(source * 256, 256), 256)
+        return pltpu.make_async_remote_copy(
+            src_ref=own.at[pl.ds(pl.multiple_of(there * 64, 64), 64)],
+            dst_ref=t_ref.at[:, columns],
+            send_sem=send_sem.at[2],
+            recv_sem=t_sem.at[source],
+            device_id={"tp": there},
+            device_id_type=pl.DeviceIdType.MESH,
+        )
+
+    for there in (y_far, y_up, y_down):
+        rows(y, there).start()
+    t_ref[:, pl.ds(pl.multiple_of(y * 256, 256), 256)] = own[
+        pl.ds(pl.multiple_of(y * 64, 64), 64), :
+    ]
+    everything = kv.at[pl.ds(0, 63)]
+    pltpu.make_async_copy(everything, everything, send_sem.at[0]).wait()
+    share(y_far, y_up).wait_recv()
+    three = whole_ref.at[pl.ds(0, 768)]
+    pltpu.make_async_copy(three, three, send_sem.at[1]).wait()
+    for there in (y_down, y_up, y_far):
+        rows(there, y_up).wait_recv()
+    three = own.at[pl.ds(0, 192)]
+    pltpu.make_async_copy(three, three, send_sem.at[2]).wait()
+
+
+def attention(queries, keys, values, query_gain, key_gain, cosine, sine, out_rows):
     vmem = pl.BlockSpec(memory_space=pltpu.VMEM)
     return pl.pallas_call(
         attention_kernel,
-        out_shape=jax.ShapeDtypeStruct((256, 256), jnp.bfloat16),
-        in_specs=[vmem] * 7,
-        out_specs=vmem,
+        out_shape=(
+            jax.ShapeDtypeStruct((64, 1024), jnp.bfloat16),
+            jax.ShapeDtypeStruct((1024, 2048), jnp.bfloat16),
+        ),
+        in_specs=[vmem] * 8,
+        out_specs=(vmem, vmem),
         scratch_shapes=[
             pltpu.VMEM((2 * CHIPS, 2, 2 * HALF, 128), jnp.bfloat16),
             pltpu.VMEM((2, 128, 512), jnp.bfloat16),
             pltpu.VMEM((2, 1, 512), jnp.float32),
             pltpu.VMEM((2, 1, 512), jnp.float32),
             pltpu.VMEM((2, 64, 512), jnp.float32),
-            pltpu.SemaphoreType.DMA((2,)),
-            pltpu.SemaphoreType.DMA((2 * CHIPS, 2)),
+            pltpu.VMEM((256, 256), jnp.bfloat16),
+            pltpu.SemaphoreType.DMA((3,)),
+            pltpu.SemaphoreType.DMA((2 * CHIPS,)),
+            pltpu.SemaphoreType.DMA((NY,)),
+            pltpu.SemaphoreType.DMA((NY,)),
         ],
         compiler_params=pltpu.CompilerParams(
             collective_id=0, has_side_effects=True, vmem_limit_bytes=40 * 2**20
@@ -222,7 +278,300 @@
             flops=8 * 10**9, bytes_accessed=2**20, transcendentals=2**24
         ),
         name="attention",
-    )(queries, keys, values, query_gain, key_gain, cosine, sine)
+    )(queries, keys, values, query_gain, key_gain, cosine, sine, out_rows)
+
+
+def places():
+    me = lax.axis_index("sp")
+    core, x, z = me % 2, (me // 2) % NX, me // (2 * NX)
+
+    def there(position, sign):
+        g, dx, dc = position // 8, (position // 2) % 4, position % 2
+        dz = (1 - 2 * (g % 2)) * ((g + 1) // 2)
+        zz, xx = (z + sign * dz + NZ) % NZ, (x + sign * dx + NX) % NX
+        return (zz * NX + xx) * 2 + (core + dc) % 2
+
+    return me, core, lax.axis_index("tp"), there
+
+
+def meet_all(there, y):
+    barrier = pltpu.get_barrier_semaphore()
+
+    def greet(p, carry):
+        pl.semaphore_signal(
+            barrier, inc=1, device_id={"sp": there(p, 1)}, device_id_type=pl.DeviceIdType.MESH
+        )
+        return carry
+
+    lax.fori_loop(1, 64, greet, 0)
+    for other in ((y + 1) % NY, (y + 3) % NY):
+        pl.semaphore_signal(
+            barrier, inc=1, device_id={"tp": other}, device_id_type=pl.DeviceIdType.MESH
+        )
+    return barrier
+
+
+def swap_matrix():
+    r = lax.broadcasted_iota(jnp.int32, (256, 256), 0)
+    c = lax.broadcasted_iota(jnp.int32, (256, 256), 1)
+    hit = (r // 16 == c % 16) & (r % 16 == c // 16)
+    return jnp.where(hit, 1.0, 0.0).astype(jnp.bfloat16)
+
+
+def to_tiles(swap, rows):
+    stacked = jnp.concatenate([rows[:, j * 128 : (j + 1) * 128] for j in range(16)], axis=0)
+    return jnp.dot(swap, stacked, preferred_element_type=jnp.float32).astype(jnp.bfloat16)
+
+
+def from_tiles(swap, tiles, out_ref, first):
+    stacked = jnp.dot(swap, tiles, preferred_element_type=jnp.float32).astype(jnp.bfloat16)
+    for j in range(16):
+        out_ref[pl.ds(first, 16), j * 128 : (j + 1) * 128] = stacked[j * 16 : (j + 1) * 16]
+
+
+def block(position):
+    return pl.ds(pl.multiple_of(position * 48, 16), 48)
+
+
+def remote(src, dst, send, recv, **where):
+    return pltpu.make_async_remote_copy(
+        src_ref=src,
+        dst_ref=dst,
+        send_sem=send,
+        recv_sem=recv,
+        device_id=where,
+        device_id_type=pl.DeviceIdType.MESH,
+    )
+
+
+def dispatch_kernel(out_ref, x_ref, packed, rows, send_sem, recv_sem, y_sem):
+    me, core, y, there = places()
+    y_up, y_down = (y + 1) % NY, (y + 3) % NY
+    barrier = meet_all(there, y)
+    swap = swap_matrix()
+
+    def pack(s, carry):
+        first = pl.multiple_of(s * 16, 16)
+        packed[pl.ds(pl.multiple_of(s * 256, 256), 256), :] = to_tiles(
+            swap, out_ref[pl.ds(first, 16), :]
+        )
+        return carry
+
+    lax.fori_loop(0, 12, pack, 0)
+    rows[0:48, :] = packed[block(me), :]
+    pl.semaphore_wait(barrier, 65)
+
+    def hand_out(p, carry):
+        to = there(p, 1)
+        remote(
+            packed.at[block(to)], rows.at[block(p)], send_sem.at[0], recv_sem.at[p], sp=to
+        ).start()
+        return carry
+
+    lax.fori_loop(1, 64, hand_out, 0)
+
+    def await_row(p, carry):
+        remote(
+            packed.at[block(p)], rows.at[block(p)], send_sem.at[0], recv_sem.at[p], sp=me
+        ).wait_recv()
+        return carry
+
+    def part(relative, k):
+        return rows.at[pl.ds(pl.multiple_of(relative * 3072 + k * 768, 256), 768)]
+
+    def along(relative_from, relative_to, k, to):
+        return remote(
+            part(relative_from, k), part(relative_to, k),
+            send_sem.at[1], y_sem.at[relative_to, k], tp=to,
+        )
+
+    def pass_on(k):
+        along(0, 1, k, y_up).wait_recv()
+        along(0, 3, k, y_down).wait_recv()
+
+        @pl.when(core == 0)
+        def _():
+            along(1, 2, k, y_up).start()
+
+        @pl.when(core == 1)
+        def _():
+            along(3, 2, k, y_down).start()
+
+    def spread(k, carry):
+        lax.fori_loop(jnp.maximum(16 * k, 1), 16 * k + 16, await_row, 0)
+        along(0, 1, k, y_up).start()
+        along(0, 3, k, y_down).start()
+
+        @pl.when(k > 0)
+        def _():
+            pass_on(k - 1)
+
+        return carry
+
+    lax.fori_loop(0, 4, spread, 0)
+    pass_on(3)
+
+    def unpack(s, carry):
+        tiles = rows[pl.ds(pl.multiple_of(s * 256, 256), 256), :]
+        from_tiles(swap, tiles, x_ref, pl.multiple_of(s * 16, 16))
+        return carry
+
+    lax.fori_loop(0, 24, unpack, 0)
+    lax.fori_loop(36, 48, unpack, 0)
+    for k in range(4):
+        along(0, 2, k, y_up).wait_recv()
+    lax.fori_loop(24, 36, unpack, 0)
+    sent = packed.at[pl.ds(0, 63 * 48)]
+    pltpu.make_async_copy(sent, sent, send_sem.at[0]).wait()
+    sent = rows.at[pl.ds(0, 9216)]
+    pltpu.make_async_copy(sent, sent, send_sem.at[1]).wait()
+
+
+def dispatch(outgoing):
+    vmem = pl.BlockSpec(memory_space=pltpu.VMEM)
+    return pl.pallas_call(
+        dispatch_kernel,
+        out_shape=jax.ShapeDtypeStruct((768, 2048), jnp.bfloat16),
+        in_specs=[vmem],
+        out_specs=vmem,
+        scratch_shapes=[
+            pltpu.VMEM((3072, 128), jnp.bfloat16),
+            pltpu.VMEM((12288, 128), jnp.bfloat16),
+            pltpu.SemaphoreType.DMA((2,)),
+            pltpu.SemaphoreType.DMA((64,)),
+            pltpu.SemaphoreType.DMA((NY, 4)),
+        ],
+        compiler_params=pltpu.CompilerParams(
+            collective_id=1, has_side_effects=True, vmem_limit_bytes=24 * 2**20
+        ),
+        name="dispatch",
+    )(outgoing)
+
+
+def combine_kernel(
+    p_ref, back_ref, far, near, both, summed, packed, returned, send_sem, recv_sem, y_sem
+):
+    me, core, y, there = places()
+    ahead, behind = (y + 1 + 2 * core) % NY, (y + 3 - 2 * core) % NY
+    to_ahead, to_behind = 3 - 2 * core, 1 + 2 * core
+    barrier = meet_all(there, y)
+    swap = swap_matrix()
+    pl.semaphore_wait(barrier, 65)
+
+    def chunk(k):
+        return pl.ds(pl.multiple_of(k * 48, 16), 48)
+
+    def partial(relative, k):
+        return pl.ds(pl.multiple_of(relative * 192 + k * 48, 16), 48)
+
+    def send_far(k):
+        return remote(
+            p_ref.at[partial(2, k)], far.at[chunk(k)], send_sem.at[0], y_sem.at[0, k], tp=ahead
+        )
+
+    def send_near(k):
+        return remote(
+            p_ref.at[partial(to_behind, k)], near.at[chunk(k)],
+            send_sem.at[0], y_sem.at[1, k], tp=behind,
+        )
+
+    def send_both(k):
+        return remote(
+            summed.at[chunk(k)], both.at[chunk(k)], send_sem.at[0], y_sem.at[2, k], tp=ahead
+        )
+
+    def send_back(p):
+        return remote(
+            packed.at[block(p)], returned.at[block(me)], send_sem.at[1], recv_sem.at[p],
+            sp=there(p, -1),
+        )
+
+    for k in range(4):
+        send_far(k).start()
+        send_near(k).start()
+
+    def finish(k):
+        send_near(k).wait_recv()
+        send_both(k).wait_recv()
+
+        def pack(s, carry):
+            first = pl.ds(pl.multiple_of(k * 48 + s * 16, 16), 16)
+            answer = (
+                p_ref[first, :].astype(jnp.float32)
+                + near[first, :].astype(jnp.float32)
+                + both[first, :].astype(jnp.float32)
+            ).astype(jnp.bfloat16)
+            packed[pl.ds(pl.multiple_of(k * 768 + s * 256, 256), 256), :] = to_tiles(swap, answer)
+            return carry
+
+        lax.fori_loop(0, 3, pack, 0)
+
+        def give_back(p, carry):
+            send_back(p).start()
+            return carry
+
+        lax.fori_loop(jnp.maximum(16 * k, 1), 16 * k + 16, give_back, 0)
+
+    def reduce(k, carry):
+        send_far(k).wait_recv()
+        summed[chunk(k), :] = (
+            p_ref[partial(to_ahead, k), :].astype(jnp.float32)
+            + far[chunk(k), :].astype(jnp.float32)
+        ).astype(jnp.bfloat16)
+        send_both(k).start()
+
+        @pl.when(k > 0)
+        def _():
+            finish(k - 1)
+
+        return carry
+
+    lax.fori_loop(0, 4, reduce, 0)
+    finish(3)
+    returned[block(me), :] = packed[0:48, :]
+
+    def await_row(p, carry):
+        source = there(p, 1)
+        remote(
+            packed.at[block(p)], returned.at[block(source)], send_sem.at[1], recv_sem.at[p], sp=source
+        ).wait_recv()
+        return carry
+
+    lax.fori_loop(1, 64, await_row, 0)
+
+    def unpack(s, carry):
+        tiles = returned[pl.ds(pl.multiple_of(s * 256, 256), 256), :]
+        from_tiles(swap, tiles, back_ref, pl.multiple_of(s * 16, 16))
+        return carry
+
+    lax.fori_loop(0, 12, unpack, 0)
+    sent = p_ref.at[pl.ds(0, 576)]
+    pltpu.make_async_copy(sent, sent, send_sem.at[0]).wait()
+    sent = packed.at[pl.ds(0, 63 * 48)]
+    pltpu.make_async_copy(sent, sent, send_sem.at[1]).wait()
+
+
+def combine(partials):
+    vmem = pl.BlockSpec(memory_space=pltpu.VMEM)
+    third = pltpu.VMEM((192, 2048), jnp.bfloat16)
+    return pl.pallas_call(
+        combine_kernel,
+        out_shape=jax.ShapeDtypeStruct((192, 2048), jnp.bfloat16),
+        in_specs=[vmem],
+        out_specs=vmem,
+        scratch_shapes=[
+            third, third, third, third,
+            pltpu.VMEM((3072, 128), jnp.bfloat16),
+            pltpu.VMEM((3072, 128), jnp.bfloat16),
+            pltpu.SemaphoreType.DMA((2,)),
+            pltpu.SemaphoreType.DMA((64,)),
+            pltpu.SemaphoreType.DMA((3, 4)),
+        ],
+        compiler_params=pltpu.CompilerParams(
+            collective_id=2, has_side_effects=True, vmem_limit_bytes=24 * 2**20
+        ),
+        name="combine",
+    )(partials)
 
 
 def local(
@@ -231,13 +580,11 @@
 ):
     head_size = query_gain.shape[0]
     seq_rows = queries.shape[0]
-    whole_out = lax.all_gather(out_rows, "tp", axis=0, tiled=True)
     cosine, sine = turn_tables(lax.axis_index("sp") * seq_rows, seq_rows, head_size)
     twice = lambda g: jnp.tile(g, 2)[None, :]
-    attended = attention(
-        queries, keys, values, twice(query_gain), twice(key_gain), cosine, sine
+    token_heads, whole_out = attention(
+        queries, keys, values, twice(query_gain), twice(key_gain), cosine, sine, out_rows
     )
-    token_heads = lax.all_to_all(attended, "tp", split_axis=0, concat_axis=1, tiled=True)
     projected = jnp.dot(token_heads, whole_out, preferred_element_type=jnp.float32)
     stream = (stream_in.astype(jnp.float32) + projected).astype(jnp.bfloat16)
     stream_wide = stream.astype(jnp.float32)
@@ -251,7 +598,7 @@
     top_count = route_ids.shape[1]
     experts = lax.axis_size("sp")
     routed = tokens * top_count
-    capacity = 3
+    capacity = SLOTS
     flat_ids = route_ids.reshape(routed)
     member = (flat_ids[:, None] == jnp.arange(experts, dtype=jnp.int32)[None, :]).astype(jnp.int32)
     earlier = jnp.cumsum(member, axis=0) - member
@@ -264,22 +611,12 @@
     outgoing = jnp.einsum("tks,td->sd", placed, normed, preferred_element_type=jnp.float32).astype(
         jnp.bfloat16
     )
-    outgoing = outgoing.reshape(experts, capacity, model_width)
-    arrived = lax.all_to_all(outgoing, "sp", split_axis=0, concat_axis=0, tiled=True)
-    flat_rows = arrived.reshape(experts * capacity, model_width)
-    row_piece = lax.all_gather(flat_rows, "tp", axis=0, tiled=True)
+    row_piece = dispatch(outgoing)
     gate_value = jnp.dot(row_piece, gate_weight[0], preferred_element_type=jnp.float32)
     up_value = jnp.dot(row_piece, up_weight[0], preferred_element_type=jnp.float32)
     hidden = (jax.nn.silu(gate_value) * up_value).astype(jnp.bfloat16)
-    summed = lax.psum_scatter(
-        jnp.dot(hidden, down_weight[0], preferred_element_type=jnp.float32).astype(jnp.bfloat16),
-        "tp",
-        scatter_dimension=0,
-        tiled=True,
-    )
-    answer = summed.reshape(experts, capacity, model_width)
-    returned = lax.all_to_all(answer, "sp", split_axis=0, concat_axis=0, tiled=True)
-    expert_back = returned.reshape(experts * capacity, model_width)
+    partials = jnp.dot(hidden, down_weight[0], preferred_element_type=jnp.float32)
+    expert_back = combine(partials.astype(jnp.bfloat16))
     picked = jnp.einsum("tks,sd->tkd", placed, expert_back, preferred_element_type=jnp.float32)
     mixed_out = stream_wide + jnp.sum(route_weights[:, :, None] * picked, axis=1)
     return mixed_out.astype(jnp.bfloat16)

time: 312 us -> 203 us (0.65)
  Pallas kernels: 83.1 us -> 173 us
  waiting for transfers between devices: 83.1 us -> 0 us
  blocking collectives: 80.1 us -> 0 us
  between operations: 13.2 us -> 0.2 us
  local copies, waits for them, and re-layouts: 18.8 us -> 10.4 us
  matrix products: 23.9 us -> 16.8 us
  starting transfers between devices: 4.82 us -> 0 us
    pallas_call x1 -> x3, Pallas kernels: 83.1 us -> 173 us  [the longest x1 63.3 us: attention(): pl.pallas_call(attention_kernel, out_shape=(jax.ShapeDtypeStruct((64, 102...]
    all_to_all x2 -> x0, blocking collectives: 80.1 us -> none  [the longest x1 41.2 us: local(): lax.all_to_all(outgoing, 'sp', split_axis=0, concat_axis=0, tiled=True)]
    reduce_scatter x1 -> x0, waiting for transfers between devices: 41.3 us -> none  [local(): lax.psum_scatter(jnp.dot(hidden, down_weight[0], preferred_element_type=j...]
    all_gather x2 -> x0, waiting for transfers between devices: 37 us -> none  [the longest x1 36.9 us: local(): row_piece = lax.all_gather(flat_rows, 'tp', axis=0, tiled=True)]
    reshape x4 -> x0, local copies, waits for them, and re-layouts: 12.9 us -> none  [the longest x1 3.28 us: local(): outgoing = outgoing.reshape(experts, capacity, model_width)]
    unnamed x17 -> x27, local copies, waits for them, and re-layouts: 3.54 us -> 8.14 us
    all_to_all x1 -> x0, starting transfers between devices: 4.59 us -> none  [local(): lax.all_to_all(attended, 'tp', split_axis=0, concat_axis=1, tiled=True)]
    all_to_all x1 -> x0, waiting for transfers between devices: 4.13 us -> none  [local(): lax.all_to_all(attended, 'tp', split_axis=0, concat_axis=1, tiled=True)]
  transfers between devices with their start and end apart: 4 -> 0, of which waited for: 3 -> 0; matrix products, arithmetic and copies ran while one was open for 1% -> 0% of each run, Pallas kernels for 27% -> 0%
where the time goes in v2:
time: 203 us
  Pallas kernels  173 us (85%)
  matrix products  16.8 us (8%)
  local copies, waits for them, and re-layouts  10.4 us (5%)
  other arithmetic  2.56 us (1%)
    pallas_call x1, Pallas kernels, attention(): pl.pallas_call(attention_kernel, out_shape=(jax.ShapeDtypeStruct((64, 102...  63.3 us
    pallas_call x1, Pallas kernels, combine(): pl.pallas_call(combine_kernel, out_shape=jax.ShapeDtypeStruct((192, 2048)...  56 us
    pallas_call x1, Pallas kernels, dispatch(): pl.pallas_call(dispatch_kernel, out_shape=jax.ShapeDtypeStruct((768, 2048...  53.8 us
    dot_general x1, matrix products, local(): jnp.dot(hidden, down_weight[0], preferred_element_type=jnp.float32)  11 us
    unnamed x27, local copies, waits for them, and re-layouts  8.14 us

profile of v2, /device:TPU:33, one launch (start us, length us, event | category | flops | bytes accessed | tf_op | source)
XLA Modules:
  0.0 203.0 jit_solution(10725364070410640500)
XLA Ops:
  0.0 0.0 copy-start
  0.0 0.8 tile.8
  0.9 0.1 broadcast_in_dim_tile.7.qg_ref
  0.9 0.7 tile.9
  1.6 0.1 broadcast_in_dim_tile.8.kg_ref
  1.7 0.1 broadcast_in_dim.48
  1.8 0.1 tile.10
  1.9 0.1 mul.70
  2.0 0.8 copy.22
  2.7 0.1 eq.44
  2.9 0.1 fusion.18
  3.0 0.2 reduce_window_sum.11
  3.2 0.2 select_reduce_fusion
  3.3 0.1 reduce_sum.39
  3.5 0.1 copy.23
  3.5 0.7 multiply_add_fusion
  4.2 0.1 convert_reduce_fusion
  4.3 0.5 sine_multiply_fusion
  4.9 0.0 copy-start.3
  4.9 1.2 copy-done.3
  6.1 0.0 copy-start.4
  6.1 0.9 copy-done.4
  7.0 0.0 copy-start.5
  7.0 0.8 copy-done.5
  7.9 0.0 copy-start.6
  7.9 0.8 copy-done.6
  8.7 0.0 copy-start.9
  8.7 63.3 %attention.1 = (bf16[64,1024]{1,0:T(8,128)(2,1)S(1)}, bf16[1024,2048]{1,0:T(8,128)(2,1)S(1)}) custom-call(bf16[256,256]{1,0:T(8,128)(2,1)S(1)} %copy-done.4, bf16[256,128]{1,0:T(8,128)(2,1)S(1)} %copy-done.5, bf16[256,128]{1,0:T(8,128)(2,1)S(1)} %copy-done.6, f32[1,128]{1,0:T(1,128)S(1)} %broadcast_in_dim_tile.7.qg_ref, ...), custom_call_target="tpu_custom_call" | custom-call | flops 8000000000 | bytes 1048576 | tf_op jit(solution)/shard_map/attention/pallas_call | solution.py:254
  72.0 0.0 copy-start.10
  72.0 0.0 copy-done.9
  72.0 1.0 multiply_reduce_fusion
  73.0 0.0 copy-start.12
  73.0 0.0 copy-done.10
  73.0 0.4 convolution_convert_fusion.1.out_ref
  73.5 53.8 %dispatch.1 = bf16[768,2048]{1,0:T(8,128)(2,1)S(1)} custom-call(bf16[192,2048]{1,0:T(8,128)(2,1)S(1)} %convolution_convert_fusion.1.out_ref), custom_call_target="tpu_custom_call" | custom-call | tf_op jit(solution)/shard_map/dispatch/pallas_call | solution.py:432
  127.2 0.0 copy-done.7
  127.2 0.0 copy-start.1
  127.2 1.6 copy-done.1
  128.9 0.0 copy-done.12
  128.9 4.0 %fusion.1 = f32[768,768]{1,0:T(8,128)} fusion(bf16[768,2048]{1,0:T(8,128)(2,1)S(1)} %dispatch.1, bf16[1,2048,768]{2,1,0:T(8,128)(2,1)S(1)} %copy-done.12), kind=kOutput, calls=%fused_computation.2 | convolution fusion | flops 2415919104 | bytes 8650752 | tf_op jit(solution)/shard_map/dot_general | solution.py:616
  132.9 0.0 copy-done
  132.9 11.0 %convolution_convert_fusion.p_ref = bf16[768,2048]{1,0:T(8,128)(2,1)} fusion(bf16[1,768,2048]{2,1,0:T(8,128)(2,1)S(1)} %copy-done, f32[768,768]{1,0:T(8,128)} %fusion.1, bf16[768,2048]{1,0:T(8,128)(2,1)} %copy-done.1, bf16[1,2048,768]{2,1,0:T(8,128)(2,1)} %param.23), kind=kOutput, calls=%fused_computation | convolution fusion | flops 4836950016 | bytes 14942208 | tf_op jit(solution)/shard_map/dot_general | solution.py:618
  143.9 1.9 copy-done.2
  145.8 56.0 %combine.1 = bf16[192,2048]{1,0:T(8,128)(2,1)S(1)} custom-call(bf16[768,2048]{1,0:T(8,128)(2,1)S(1)} %copy-done.2), custom_call_target="tpu_custom_call" | custom-call | tf_op jit(solution)/shard_map/combine/pallas_call | solution.py:557
  201.9 0.0 copy-done.11
  201.9 0.4 fusion.9
  202.3 0.0 copy-done.8
  202.3 0.8 add_convert_fusion
  (10 shorter events, 0.1 us)
Async XLA Ops:
  0.0 132.9 %copy-start = (bf16[1,768,2048]{2,1,0:T(8,128)(2,1)S(1)}, bf16[1,768,2048]{2,1,0:T(8,128)(2,1)}, u32[]{:S(2)}) copy-start(bf16[1,768,2048]{2,1,0:T(8,128)(2,1)} %param.25) | copy-start | bytes 9437188
  4.9 1.2 copy-start.3
  6.1 0.9 copy-start.4
  7.0 0.8 copy-start.5
  7.9 0.8 copy-start.6
  8.7 63.3 %copy-start.9 = (bf16[64,2048]{1,0:T(8,128)(2,1)S(1)}, bf16[64,2048]{1,0:T(8,128)(2,1)}, u32[]{:S(2)}) copy-start(bf16[64,2048]{1,0:T(8,128)(2,1)} %param.13) | copy-start | bytes 786436
  72.0 1.0 copy-start.10
  73.0 54.2 %copy-start.7 = (f32[64,2048]{1,0:T(8,128)}, f32[64,2048]{1,0:T(8,128)S(1)}, u32[]{:S(2)}) copy-start(f32[64,2048]{1,0:T(8,128)S(1)} %get-tuple-element.12) | copy-start | bytes 1572868
  73.0 55.9 %copy-start.12 = (bf16[1,2048,768]{2,1,0:T(8,128)(2,1)S(1)}, bf16[1,2048,768]{2,1,0:T(8,128)(2,1)}, u32[]{:S(2)}) copy-start(bf16[1,2048,768]{2,1,0:T(8,128)(2,1)} %param.24) | copy-start | bytes 9437188
  127.2 1.7 copy-start.1
  143.9 1.9 copy-start.2
  145.8 56.1 %copy-start.11 = (f32[64,2]{0,1:T(2,128)S(1)}, f32[64,2]{0,1:T(2,128)}, u32[]{:S(2)}) copy-start(f32[64,2]{0,1:T(2,128)} %param.22) | copy-start | bytes 1540
  145.8 56.4 %copy-start.8 = (f32[64,2048]{1,0:T(8,128)S(1)}, f32[64,2048]{1,0:T(8,128)}, u32[]{:S(2)}) copy-start(f32[64,2048]{1,0:T(8,128)} %copy-done.7) | copy-start | bytes 1572868

commit v3 on v2

--- a/solution.py
+++ b/solution.py
@@ -344,17 +344,30 @@
     )
 
 
-def dispatch_kernel(out_ref, x_ref, packed, rows, send_sem, recv_sem, y_sem):
+def experts_kernel(
+    out_ref, gate_hbm, up_hbm, down_hbm, back_ref,
+    gate, up, down, packed, rows, x_rows, hidden, parts, far, near, both, summed, answers, returned,
+    load_sem, send_sem, out_sem, spread_sem, sum_sem, back_sem,
+):
     me, core, y, there = places()
     y_up, y_down = (y + 1) % NY, (y + 3) % NY
+    ahead, behind = (y + 1 + 2 * core) % NY, (y + 3 - 2 * core) % NY
+    to_ahead, to_behind = 3 - 2 * core, 1 + 2 * core
     barrier = meet_all(there, y)
+    loads = [
+        pltpu.make_async_copy(src, dst, load_sem.at[i])
+        for i, (src, dst) in enumerate(((gate_hbm, gate), (up_hbm, up), (down_hbm, down)))
+    ]
+    for load in loads:
+        load.start()
     swap = swap_matrix()
+
+    def tiles_at(first):
+        return pl.ds(pl.multiple_of(first, 256), 256)
 
     def pack(s, carry):
         first = pl.multiple_of(s * 16, 16)
-        packed[pl.ds(pl.multiple_of(s * 256, 256), 256), :] = to_tiles(
-            swap, out_ref[pl.ds(first, 16), :]
-        )
+        packed[tiles_at(s * 256), :] = to_tiles(swap, out_ref[pl.ds(first, 16), :])
         return carry
 
     lax.fori_loop(0, 12, pack, 0)
@@ -364,17 +377,11 @@
     def hand_out(p, carry):
         to = there(p, 1)
         remote(
-            packed.at[block(to)], rows.at[block(p)], send_sem.at[0], recv_sem.at[p], sp=to
+            packed.at[block(to)], rows.at[block(p)], send_sem.at[0], out_sem.at[p], sp=to
         ).start()
         return carry
 
     lax.fori_loop(1, 64, hand_out, 0)
-
-    def await_row(p, carry):
-        remote(
-            packed.at[block(p)], rows.at[block(p)], send_sem.at[0], recv_sem.at[p], sp=me
-        ).wait_recv()
-        return carry
 
     def part(relative, k):
         return rows.at[pl.ds(pl.multiple_of(relative * 3072 + k * 768, 256), 768)]
@@ -382,8 +389,19 @@
     def along(relative_from, relative_to, k, to):
         return remote(
             part(relative_from, k), part(relative_to, k),
-            send_sem.at[1], y_sem.at[relative_to, k], tp=to,
-        )
+            send_sem.at[1], spread_sem.at[relative_to, k], tp=to,
+        )
+
+    def await_row(p, carry):
+        remote(
+            packed.at[block(p)], rows.at[block(p)], send_sem.at[0], out_sem.at[p], sp=me
+        ).wait_recv()
+        return carry
+
+    def spread(k):
+        lax.fori_loop(jnp.maximum(16 * k, 1), 16 * k + 16, await_row, 0)
+        along(0, 1, k, y_up).start()
+        along(0, 3, k, y_down).start()
 
     def pass_on(k):
         along(0, 1, k, y_up).wait_recv()
@@ -397,181 +415,171 @@
         def _():
             along(3, 2, k, y_down).start()
 
-    def spread(k, carry):
-        lax.fori_loop(jnp.maximum(16 * k, 1), 16 * k + 16, await_row, 0)
-        along(0, 1, k, y_up).start()
-        along(0, 3, k, y_down).start()
-
-        @pl.when(k > 0)
-        def _():
-            pass_on(k - 1)
-
-        return carry
-
-    lax.fori_loop(0, 4, spread, 0)
-    pass_on(3)
-
-    def unpack(s, carry):
-        tiles = rows[pl.ds(pl.multiple_of(s * 256, 256), 256), :]
-        from_tiles(swap, tiles, x_ref, pl.multiple_of(s * 16, 16))
-        return carry
-
-    lax.fori_loop(0, 24, unpack, 0)
-    lax.fori_loop(36, 48, unpack, 0)
-    for k in range(4):
-        along(0, 2, k, y_up).wait_recv()
-    lax.fori_loop(24, 36, unpack, 0)
-    sent = packed.at[pl.ds(0, 63 * 48)]
-    pltpu.make_async_copy(sent, sent, send_sem.at[0]).wait()
-    sent = rows.at[pl.ds(0, 9216)]
-    pltpu.make_async_copy(sent, sent, send_sem.at[1]).wait()
-
-
-def dispatch(outgoing):
-    vmem = pl.BlockSpec(memory_space=pltpu.VMEM)
-    return pl.pallas_call(
-        dispatch_kernel,
-        out_shape=jax.ShapeDtypeStruct((768, 2048), jnp.bfloat16),
-        in_specs=[vmem],
-        out_specs=vmem,
-        scratch_shapes=[
-            pltpu.VMEM((3072, 128), jnp.bfloat16),
-            pltpu.VMEM((12288, 128), jnp.bfloat16),
-            pltpu.SemaphoreType.DMA((2,)),
-            pltpu.SemaphoreType.DMA((64,)),
-            pltpu.SemaphoreType.DMA((NY, 4)),
-        ],
-        compiler_params=pltpu.CompilerParams(
-            collective_id=1, has_side_effects=True, vmem_limit_bytes=24 * 2**20
-        ),
-        name="dispatch",
-    )(outgoing)
-
-
-def combine_kernel(
-    p_ref, back_ref, far, near, both, summed, packed, returned, send_sem, recv_sem, y_sem
-):
-    me, core, y, there = places()
-    ahead, behind = (y + 1 + 2 * core) % NY, (y + 3 - 2 * core) % NY
-    to_ahead, to_behind = 3 - 2 * core, 1 + 2 * core
-    barrier = meet_all(there, y)
-    swap = swap_matrix()
-    pl.semaphore_wait(barrier, 65)
-
     def chunk(k):
         return pl.ds(pl.multiple_of(k * 48, 16), 48)
 
     def partial(relative, k):
-        return pl.ds(pl.multiple_of(relative * 192 + k * 48, 16), 48)
+        return pl.ds(pl.multiple_of(k * 192 + relative * 48, 16), 48)
 
     def send_far(k):
         return remote(
-            p_ref.at[partial(2, k)], far.at[chunk(k)], send_sem.at[0], y_sem.at[0, k], tp=ahead
+            parts.at[partial(2, k)], far.at[chunk(k)], send_sem.at[2], sum_sem.at[0, k], tp=ahead
         )
 
     def send_near(k):
         return remote(
-            p_ref.at[partial(to_behind, k)], near.at[chunk(k)],
-            send_sem.at[0], y_sem.at[1, k], tp=behind,
+            parts.at[partial(to_behind, k)], near.at[chunk(k)],
+            send_sem.at[2], sum_sem.at[1, k], tp=behind,
         )
 
     def send_both(k):
         return remote(
-            summed.at[chunk(k)], both.at[chunk(k)], send_sem.at[0], y_sem.at[2, k], tp=ahead
-        )
-
-    def send_back(p):
-        return remote(
-            packed.at[block(p)], returned.at[block(me)], send_sem.at[1], recv_sem.at[p],
-            sp=there(p, -1),
-        )
-
-    for k in range(4):
+            summed.at[chunk(k)], both.at[chunk(k)], send_sem.at[2], sum_sem.at[2, k], tp=ahead
+        )
+
+    def compute(k):
+        along(0, 2, k, y_up).wait_recv()
+
+        def unpack_x(i, carry):
+            relative, s = i // 3, i % 3
+            tiles = rows[tiles_at(relative * 3072 + k * 768 + s * 256), :]
+            from_tiles(swap, tiles, x_rows, pl.multiple_of(i * 16, 16))
+            return carry
+
+        lax.fori_loop(0, 12, unpack_x, 0)
+        mine = x_rows[...]
+        for n in range(3):
+            columns = slice(n * 256, (n + 1) * 256)
+            gated = jnp.dot(mine, gate[:, columns], preferred_element_type=jnp.float32)
+            upped = jnp.dot(mine, up[:, columns], preferred_element_type=jnp.float32)
+            hidden[:, columns] = (gated / (1.0 + jnp.exp(-gated)) * upped).astype(jnp.bfloat16)
+        units = hidden[...]
+        for n in range(8):
+            columns = slice(n * 256, (n + 1) * 256)
+            parts[pl.ds(pl.multiple_of(k * 192, 16), 192), columns] = jnp.dot(
+                units, down[:, columns], preferred_element_type=jnp.float32
+            ).astype(jnp.bfloat16)
         send_far(k).start()
         send_near(k).start()
+
+    def add_far(k):
+        send_far(k).wait_recv()
+        summed[chunk(k), :] = (
+            parts[partial(to_ahead, k), :].astype(jnp.float32)
+            + far[chunk(k), :].astype(jnp.float32)
+        ).astype(jnp.bfloat16)
+        send_both(k).start()
 
     def finish(k):
         send_near(k).wait_recv()
         send_both(k).wait_recv()
 
-        def pack(s, carry):
-            first = pl.ds(pl.multiple_of(k * 48 + s * 16, 16), 16)
+        def pack_answer(s, carry):
+            own = pl.ds(pl.multiple_of(k * 192 + s * 16, 16), 16)
+            arrived = pl.ds(pl.multiple_of(k * 48 + s * 16, 16), 16)
             answer = (
-                p_ref[first, :].astype(jnp.float32)
-                + near[first, :].astype(jnp.float32)
-                + both[first, :].astype(jnp.float32)
+                parts[own, :].astype(jnp.float32)
+                + near[arrived, :].astype(jnp.float32)
+                + both[arrived, :].astype(jnp.float32)
             ).astype(jnp.bfloat16)
-            packed[pl.ds(pl.multiple_of(k * 768 + s * 256, 256), 256), :] = to_tiles(swap, answer)
+            answers[tiles_at(k * 768 + s * 256), :] = to_tiles(swap, answer)
             return carry
 
-        lax.fori_loop(0, 3, pack, 0)
+        lax.fori_loop(0, 3, pack_answer, 0)
 
         def give_back(p, carry):
-            send_back(p).start()
+            remote(
+                answers.at[block(p)], returned.at[block(me)], send_sem.at[3], back_sem.at[p],
+                sp=there(p, -1),
+            ).start()
             return carry
 
         lax.fori_loop(jnp.maximum(16 * k, 1), 16 * k + 16, give_back, 0)
 
-    def reduce(k, carry):
-        send_far(k).wait_recv()
-        summed[chunk(k), :] = (
-            p_ref[partial(to_ahead, k), :].astype(jnp.float32)
-            + far[chunk(k), :].astype(jnp.float32)
-        ).astype(jnp.bfloat16)
-        send_both(k).start()
-
-        @pl.when(k > 0)
-        def _():
-            finish(k - 1)
-
-        return carry
-
-    lax.fori_loop(0, 4, reduce, 0)
-    finish(3)
-    returned[block(me), :] = packed[0:48, :]
-
-    def await_row(p, carry):
+    def tick(t, carry):
+        @pl.when(t < 4)
+        def _():
+            spread(t)
+
+        @pl.when((t >= 1) & (t < 5))
+        def _():
+            pass_on(t - 1)
+
+        @pl.when(t == 2)
+        def _():
+            for load in loads:
+                load.wait()
+
+        @pl.when((t >= 3) & (t < 7))
+        def _():
+            add_far(t - 3)
+
+        @pl.when((t >= 2) & (t < 6))
+        def _():
+            compute(t - 2)
+
+        @pl.when(t >= 4)
+        def _():
+            finish(t - 4)
+
+        return carry
+
+    lax.fori_loop(0, 8, tick, 0)
+    returned[block(me), :] = answers[0:48, :]
+
+    def await_back(p, carry):
         source = there(p, 1)
         remote(
-            packed.at[block(p)], returned.at[block(source)], send_sem.at[1], recv_sem.at[p], sp=source
+            answers.at[block(p)], returned.at[block(source)], send_sem.at[3], back_sem.at[p],
+            sp=source,
         ).wait_recv()
         return carry
 
-    lax.fori_loop(1, 64, await_row, 0)
+    lax.fori_loop(1, 64, await_back, 0)
 
     def unpack(s, carry):
-        tiles = returned[pl.ds(pl.multiple_of(s * 256, 256), 256), :]
-        from_tiles(swap, tiles, back_ref, pl.multiple_of(s * 16, 16))
+        from_tiles(swap, returned[tiles_at(s * 256), :], back_ref, pl.multiple_of(s * 16, 16))
         return carry
 
     lax.fori_loop(0, 12, unpack, 0)
-    sent = p_ref.at[pl.ds(0, 576)]
-    pltpu.make_async_copy(sent, sent, send_sem.at[0]).wait()
-    sent = packed.at[pl.ds(0, 63 * 48)]
-    pltpu.make_async_copy(sent, sent, send_sem.at[1]).wait()
-
-
-def combine(partials):
+    for i, sent in enumerate((
+        packed.at[pl.ds(0, 63 * 48)],
+        rows.at[pl.ds(0, 9216)],
+        parts.at[pl.ds(0, 576)],
+        answers.at[pl.ds(0, 63 * 48)],
+    )):
+        pltpu.make_async_copy(sent, sent, send_sem.at[i]).wait()
+
+
+def expert_layer(outgoing, gate, up, down):
     vmem = pl.BlockSpec(memory_space=pltpu.VMEM)
-    third = pltpu.VMEM((192, 2048), jnp.bfloat16)
+    hbm = pl.BlockSpec(memory_space=pltpu.HBM)
+
+    def room(*shape):
+        return pltpu.VMEM(shape, jnp.bfloat16)
+
     return pl.pallas_call(
-        combine_kernel,
+        experts_kernel,
         out_shape=jax.ShapeDtypeStruct((192, 2048), jnp.bfloat16),
-        in_specs=[vmem],
+        in_specs=[vmem, hbm, hbm, hbm],
         out_specs=vmem,
         scratch_shapes=[
-            third, third, third, third,
-            pltpu.VMEM((3072, 128), jnp.bfloat16),
-            pltpu.VMEM((3072, 128), jnp.bfloat16),
-            pltpu.SemaphoreType.DMA((2,)),
+            room(2048, 768), room(2048, 768), room(768, 2048),
+            room(3072, 128), room(12288, 128), room(192, 2048), room(192, 768), room(768, 2048),
+            room(192, 2048), room(192, 2048), room(192, 2048), room(192, 2048),
+            room(3072, 128), room(3072, 128),
+            pltpu.SemaphoreType.DMA((3,)),
+            pltpu.SemaphoreType.DMA((4,)),
             pltpu.SemaphoreType.DMA((64,)),
+            pltpu.SemaphoreType.DMA((NY, 4)),
             pltpu.SemaphoreType.DMA((3, 4)),
+            pltpu.SemaphoreType.DMA((64,)),
         ],
         compiler_params=pltpu.CompilerParams(
-            collective_id=2, has_side_effects=True, vmem_limit_bytes=24 * 2**20
+            collective_id=1, has_side_effects=True, vmem_limit_bytes=56 * 2**20
         ),
-        name="combine",
-    )(partials)
+        name="experts",
+    )(outgoing, gate, up, down)
 
 
 def local(
@@ -611,12 +619,7 @@
     outgoing = jnp.einsum("tks,td->sd", placed, normed, preferred_element_type=jnp.float32).astype(
         jnp.bfloat16
     )
-    row_piece = dispatch(outgoing)
-    gate_value = jnp.dot(row_piece, gate_weight[0], preferred_element_type=jnp.float32)
-    up_value = jnp.dot(row_piece, up_weight[0], preferred_element_type=jnp.float32)
-    hidden = (jax.nn.silu(gate_value) * up_value).astype(jnp.bfloat16)
-    partials = jnp.dot(hidden, down_weight[0], preferred_element_type=jnp.float32)
-    expert_back = combine(partials.astype(jnp.bfloat16))
+    expert_back = expert_layer(outgoing, gate_weight[0], up_weight[0], down_weight[0])
     picked = jnp.einsum("tks,sd->tkd", placed, expert_back, preferred_element_type=jnp.float32)
     mixed_out = stream_wide + jnp.sum(route_weights[:, :, None] * picked, axis=1)
     return mixed_out.astype(jnp.bfloat16)

time: 203 us -> 176 us (0.87)
  matrix products: 16.8 us -> 3.78 us
  Pallas kernels: 173 us -> 163 us
  local copies, waits for them, and re-layouts: 10.4 us -> 6 us
    dot_general x2 -> x0, matrix products: 15 us -> none  [the longest x1 11 us: local(): jnp.dot(hidden, down_weight[0], preferred_element_type=jnp.float32)]
    pallas_call x2 -> x1, Pallas kernels: 110 us -> 100 us  [expert_layer(): pl.pallas_call(experts_kernel, out_shape=jax.ShapeDtypeStruct((192, 2048)...]
    unnamed x27 -> x17, local copies, waits for them, and re-layouts: 8.14 us -> 3.92 us
where the time goes in v3:
time: 176 us; the launch traced here: 175 us
  Pallas kernels  163 us (93%)
  local copies, waits for them, and re-layouts  6 us (3%)
  matrix products  3.78 us (2%)
  other arithmetic  1.89 us (1%)
    pallas_call x1, Pallas kernels, expert_layer(): pl.pallas_call(experts_kernel, out_shape=jax.ShapeDtypeStruct((192, 2048)...  100 us
    pallas_call x1, Pallas kernels, attention(): pl.pallas_call(attention_kernel, out_shape=(jax.ShapeDtypeStruct((64, 102...  63.3 us
    unnamed x17, local copies, waits for them, and re-layouts  3.92 us

profile of v3, /device:TPU:33, one launch (start us, length us, event | category | flops | bytes accessed | tf_op | source)
XLA Modules:
  0.0 175.3 jit_solution(16025546862064368109)
XLA Ops:
  0.0 0.1 broadcast_in_dim.48
  0.1 0.1 tile.10
  0.2 0.1 mul.63
  0.3 0.5 sine_multiply_fusion
  0.9 0.7 tile.8
  1.5 0.1 broadcast_in_dim_tile.7.qg_ref
  1.6 0.7 tile.9
  2.3 0.1 broadcast_in_dim_tile.8.kg_ref
  2.3 0.0 copy-start
  2.3 1.2 copy-done
  3.6 0.0 copy-start.1
  3.6 0.9 copy-done.1
  4.5 0.0 copy-start.2
  4.5 0.8 copy-done.2
  5.3 0.0 copy-start.3
  5.3 0.8 copy-done.3
  6.2 0.0 copy-start.4
  6.2 63.3 %attention.1 = (bf16[64,1024]{1,0:T(8,128)(2,1)S(1)}, bf16[1024,2048]{1,0:T(8,128)(2,1)S(1)}) custom-call(bf16[256,256]{1,0:T(8,128)(2,1)S(1)} %copy-done.1, bf16[256,128]{1,0:T(8,128)(2,1)S(1)} %copy-done.2, bf16[256,128]{1,0:T(8,128)(2,1)S(1)} %copy-done.3, f32[1,128]{1,0:T(1,128)S(1)} %broadcast_in_dim_tile.7.qg_ref, ...), custom_call_target="tpu_custom_call" | custom-call | flops 8000000000 | bytes 1048576 | tf_op jit(solution)/shard_map/attention/pallas_call | solution.py:254
  69.5 0.0 copy-start.6
  69.5 0.0 copy-start.5
  69.5 0.0 copy-done.4
  69.5 1.0 multiply_reduce_fusion
  70.5 0.0 copy-done.6
  70.5 0.1 copy.22
  70.6 0.1 eq.44
  70.7 0.1 fusion.9
  70.8 0.2 reduce_window_sum.11
  71.0 0.2 select_reduce_fusion
  71.2 0.1 reduce_sum.39
  71.3 0.1 copy.23
  71.4 0.1 convert_reduce_fusion
  71.5 0.0 copy-done.5
  71.5 1.3 convolution_convert_fusion.out_ref
  72.8 0.0 copy-start.7
  72.8 100.1 %experts.1 = bf16[192,2048]{1,0:T(8,128)(2,1)} custom-call(bf16[192,2048]{1,0:T(8,128)(2,1)} %convolution_convert_fusion.out_ref, bf16[2048,768]{1,0:T(8,128)(2,1)} %bitcast.9, bf16[2048,768]{1,0:T(8,128)(2,1)} %bitcast.10, bf16[768,2048]{1,0:T(8,128)(2,1)} %bitcast.11), custom_call_target="tpu_custom_call" | custom-call | tf_op jit(solution)/shard_map/experts/pallas_call | solution.py:561
  173.0 0.0 copy-done.7
  173.0 1.5 fusion.2
  174.5 0.8 add_convert_fusion
  (7 shorter events, 0.1 us)
Async XLA Ops:
  2.3 1.2 copy-start
  3.6 0.9 copy-start.1
  4.5 0.8 copy-start.2
  5.3 0.8 copy-start.3
  6.2 63.3 %copy-start.4 = (bf16[64,2048]{1,0:T(8,128)(2,1)S(1)}, bf16[64,2048]{1,0:T(8,128)(2,1)}, u32[]{:S(2)}) copy-start(bf16[64,2048]{1,0:T(8,128)(2,1)} %param.13) | copy-start | bytes 786436
  69.5 1.0 copy-start.6
  69.5 2.0 %copy-start.5 = (f32[2048]{0:T(1024)S(1)}, f32[2048]{0:T(1024)}, u32[]{:S(2)}) copy-start(f32[2048]{0:T(1024)} %param.20) | copy-start | bytes 24580
  72.8 100.2 %copy-start.7 = (f32[64,2]{0,1:T(2,128)S(1)}, f32[64,2]{0,1:T(2,128)}, u32[]{:S(2)}) copy-start(f32[64,2]{0,1:T(2,128)} %param.22) | copy-start | bytes 1540

commit v4 on v3

--- a/solution.py
+++ b/solution.py
@@ -12,7 +12,7 @@
 CHIPS = NZ * NX
 CHUNK = 1
 AHEAD = 3
-WEIGHTS_AT = 16
+WEIGHTS_AT = 20
 SLOTS = 3
 HALF = 128
 
@@ -374,14 +374,19 @@
     rows[0:48, :] = packed[block(me), :]
     pl.semaphore_wait(barrier, 65)
 
-    def hand_out(p, carry):
+    def hand_out(i, carry):
+        p = (i + 16) % 64
         to = there(p, 1)
-        remote(
-            packed.at[block(to)], rows.at[block(p)], send_sem.at[0], out_sem.at[p], sp=to
-        ).start()
-        return carry
-
-    lax.fori_loop(1, 64, hand_out, 0)
+
+        @pl.when(p > 0)
+        def _():
+            remote(
+                packed.at[block(to)], rows.at[block(p)], send_sem.at[0], out_sem.at[p], sp=to
+            ).start()
+
+        return carry
+
+    lax.fori_loop(0, 64, hand_out, 0)
 
     def part(relative, k):
         return rows.at[pl.ds(pl.multiple_of(relative * 3072 + k * 768, 256), 768)]
@@ -499,28 +504,28 @@
     def tick(t, carry):
         @pl.when(t < 4)
         def _():
-            spread(t)
+            spread((t + 1) % 4)
 
         @pl.when((t >= 1) & (t < 5))
         def _():
-            pass_on(t - 1)
+            pass_on(t % 4)
 
         @pl.when(t == 2)
         def _():
             for load in loads:
                 load.wait()
 
+        @pl.when((t >= 2) & (t < 6))
+        def _():
+            compute((t - 1) % 4)
+
         @pl.when((t >= 3) & (t < 7))
         def _():
-            add_far(t - 3)
-
-        @pl.when((t >= 2) & (t < 6))
-        def _():
-            compute(t - 2)
+            add_far((t - 2) % 4)
 
         @pl.when(t >= 4)
         def _():
-            finish(t - 4)
+            finish((t - 3) % 4)
 
         return carry
 

time: 176 us -> 171 us (0.972)
  Pallas kernels: 163 us -> 159 us
    pallas_call x1, Pallas kernels: 100 us -> 95.6 us  [expert_layer(): pl.pallas_call(experts_kernel, out_shape=jax.ShapeDtypeStruct((192, 2048)...]
where the time goes in v4:
time: 171 us
  Pallas kernels  159 us (93%)
  local copies, waits for them, and re-layouts  6 us (4%)
  matrix products  3.78 us (2%)
  other arithmetic  1.89 us (1%)
    pallas_call x1, Pallas kernels, expert_layer(): pl.pallas_call(experts_kernel, out_shape=jax.ShapeDtypeStruct((192, 2048)...  95.6 us
    pallas_call x1, Pallas kernels, attention(): pl.pallas_call(attention_kernel, out_shape=(jax.ShapeDtypeStruct((64, 102...  63.3 us
    unnamed x17, local copies, waits for them, and re-layouts  3.92 us

profile of v4, /device:TPU:33, one launch (start us, length us, event | category | flops | bytes accessed | tf_op | source)
XLA Modules:
  0.0 170.7 jit_solution(7962285192053438399)
XLA Ops:
  0.0 0.1 broadcast_in_dim.48
  0.1 0.1 tile.10
  0.2 0.1 mul.63
  0.3 0.5 sine_multiply_fusion
  0.9 0.7 tile.8
  1.5 0.1 broadcast_in_dim_tile.7.qg_ref
  1.6 0.7 tile.9
  2.3 0.1 broadcast_in_dim_tile.8.kg_ref
  2.3 0.0 copy-start
  2.3 1.2 copy-done
  3.6 0.0 copy-start.1
  3.6 0.9 copy-done.1
  4.5 0.0 copy-start.2
  4.5 0.8 copy-done.2
  5.3 0.0 copy-start.3
  5.3 0.8 copy-done.3
  6.2 0.0 copy-start.4
  6.2 63.3 %attention.1 = (bf16[64,1024]{1,0:T(8,128)(2,1)S(1)}, bf16[1024,2048]{1,0:T(8,128)(2,1)S(1)}) custom-call(bf16[256,256]{1,0:T(8,128)(2,1)S(1)} %copy-done.1, bf16[256,128]{1,0:T(8,128)(2,1)S(1)} %copy-done.2, bf16[256,128]{1,0:T(8,128)(2,1)S(1)} %copy-done.3, f32[1,128]{1,0:T(1,128)S(1)} %broadcast_in_dim_tile.7.qg_ref, ...), custom_call_target="tpu_custom_call" | custom-call | flops 8000000000 | bytes 1048576 | tf_op jit(solution)/shard_map/attention/pallas_call | solution.py:254
  69.5 0.0 copy-start.6
  69.5 0.0 copy-start.5
  69.5 0.0 copy-done.4
  69.5 1.0 multiply_reduce_fusion
  70.5 0.0 copy-done.6
  70.5 0.1 copy.22
  70.6 0.1 eq.44
  70.7 0.1 fusion.9
  70.8 0.2 reduce_window_sum.11
  71.0 0.2 select_reduce_fusion
  71.2 0.1 reduce_sum.39
  71.3 0.1 copy.23
  71.4 0.1 convert_reduce_fusion
  71.5 0.0 copy-done.5
  71.5 1.3 convolution_convert_fusion.out_ref
  72.8 0.0 copy-start.7
  72.8 95.6 %experts.1 = bf16[192,2048]{1,0:T(8,128)(2,1)} custom-call(bf16[192,2048]{1,0:T(8,128)(2,1)} %convolution_convert_fusion.out_ref, bf16[2048,768]{1,0:T(8,128)(2,1)} %bitcast.9, bf16[2048,768]{1,0:T(8,128)(2,1)} %bitcast.10, bf16[768,2048]{1,0:T(8,128)(2,1)} %bitcast.11), custom_call_target="tpu_custom_call" | custom-call | tf_op jit(solution)/shard_map/experts/pallas_call | solution.py:566
  168.4 0.0 copy-done.7
  168.5 1.5 fusion.2
  170.0 0.8 add_convert_fusion
  (7 shorter events, 0.1 us)
Async XLA Ops:
  2.3 1.2 copy-start
  3.6 0.9 copy-start.1
  4.5 0.8 copy-start.2
  5.3 0.8 copy-start.3
  6.2 63.3 %copy-start.4 = (bf16[64,2048]{1,0:T(8,128)(2,1)S(1)}, bf16[64,2048]{1,0:T(8,128)(2,1)}, u32[]{:S(2)}) copy-start(bf16[64,2048]{1,0:T(8,128)(2,1)} %param.13) | copy-start | bytes 786436
  69.5 1.0 copy-start.6
  69.5 2.0 %copy-start.5 = (f32[2048]{0:T(1024)S(1)}, f32[2048]{0:T(1024)}, u32[]{:S(2)}) copy-start(f32[2048]{0:T(1024)} %param.20) | copy-start | bytes 24580
  72.8 95.6 %copy-start.7 = (f32[64,2]{0,1:T(2,128)S(1)}, f32[64,2]{0,1:T(2,128)}, u32[]{:S(2)}) copy-start(f32[64,2]{0,1:T(2,128)} %param.22) | copy-start | bytes 1540

commit v5 on v4

--- a/solution.py
+++ b/solution.py
@@ -11,7 +11,7 @@
 NZ, NX, NY = 8, 4, 4
 CHIPS = NZ * NX
 CHUNK = 1
-AHEAD = 3
+AHEAD = 4
 WEIGHTS_AT = 20
 SLOTS = 3
 HALF = 128

time: 171 us -> 170 us (level)
  no operation moved by 1% of the time
where the time goes in v5:
time: 170 us
  Pallas kernels  158 us (93%)
  local copies, waits for them, and re-layouts  6 us (4%)
  matrix products  3.78 us (2%)
  other arithmetic  1.89 us (1%)
    pallas_call x1, Pallas kernels, expert_layer(): pl.pallas_call(experts_kernel, out_shape=jax.ShapeDtypeStruct((192, 2048)...  94 us
    pallas_call x1, Pallas kernels, attention(): pl.pallas_call(attention_kernel, out_shape=(jax.ShapeDtypeStruct((64, 102...  64.3 us
    unnamed x17, local copies, waits for them, and re-layouts  3.92 us

profile of v5, /device:TPU:33, one launch (start us, length us, event | category | flops | bytes accessed | tf_op | source)
XLA Modules:
  0.0 170.2 jit_solution(18142721855027348188)
XLA Ops:
  0.0 0.1 broadcast_in_dim.48
  0.1 0.1 tile.10
  0.2 0.1 mul.63
  0.3 0.5 sine_multiply_fusion
  0.9 0.7 tile.8
  1.5 0.1 broadcast_in_dim_tile.7.qg_ref
  1.6 0.7 tile.9
  2.3 0.1 broadcast_in_dim_tile.8.kg_ref
  2.3 0.0 copy-start
  2.3 1.2 copy-done
  3.6 0.0 copy-start.1
  3.6 0.9 copy-done.1
  4.5 0.0 copy-start.2
  4.5 0.8 copy-done.2
  5.3 0.0 copy-start.3
  5.3 0.8 copy-done.3
  6.2 0.0 copy-start.4
  6.2 64.3 %attention.1 = (bf16[64,1024]{1,0:T(8,128)(2,1)S(1)}, bf16[1024,2048]{1,0:T(8,128)(2,1)S(1)}) custom-call(bf16[256,256]{1,0:T(8,128)(2,1)S(1)} %copy-done.1, bf16[256,128]{1,0:T(8,128)(2,1)S(1)} %copy-done.2, bf16[256,128]{1,0:T(8,128)(2,1)S(1)} %copy-done.3, f32[1,128]{1,0:T(1,128)S(1)} %broadcast_in_dim_tile.7.qg_ref, ...), custom_call_target="tpu_custom_call" | custom-call | flops 8000000000 | bytes 1048576 | tf_op jit(solution)/shard_map/attention/pallas_call | solution.py:254
  70.5 0.0 copy-start.6
  70.5 0.0 copy-start.5
  70.5 0.0 copy-done.4
  70.5 1.0 multiply_reduce_fusion
  71.5 0.0 copy-done.6
  71.5 0.1 copy.22
  71.6 0.1 eq.44
  71.7 0.1 fusion.9
  71.8 0.2 reduce_window_sum.11
  72.0 0.2 select_reduce_fusion
  72.2 0.1 reduce_sum.39
  72.3 0.1 copy.23
  72.4 0.1 convert_reduce_fusion
  72.5 0.0 copy-done.5
  72.5 1.3 convolution_convert_fusion.out_ref
  73.8 0.0 copy-start.7
  73.8 94.0 %experts.1 = bf16[192,2048]{1,0:T(8,128)(2,1)} custom-call(bf16[192,2048]{1,0:T(8,128)(2,1)} %convolution_convert_fusion.out_ref, bf16[2048,768]{1,0:T(8,128)(2,1)} %bitcast.9, bf16[2048,768]{1,0:T(8,128)(2,1)} %bitcast.10, bf16[768,2048]{1,0:T(8,128)(2,1)} %bitcast.11), custom_call_target="tpu_custom_call" | custom-call | tf_op jit(solution)/shard_map/experts/pallas_call | solution.py:566
  167.9 0.0 copy-done.7
  167.9 1.5 fusion.2
  169.4 0.8 add_convert_fusion
  (7 shorter events, 0.1 us)
Async XLA Ops:
  2.3 1.2 copy-start
  3.6 0.9 copy-start.1
  4.5 0.8 copy-start.2
  5.3 0.8 copy-start.3
  6.2 64.3 %copy-start.4 = (bf16[64,2048]{1,0:T(8,128)(2,1)S(1)}, bf16[64,2048]{1,0:T(8,128)(2,1)}, u32[]{:S(2)}) copy-start(bf16[64,2048]{1,0:T(8,128)(2,1)} %param.13) | copy-start | bytes 786436
  70.5 1.0 copy-start.6
  70.5 2.0 %copy-start.5 = (f32[2048]{0:T(1024)S(1)}, f32[2048]{0:T(1024)}, u32[]{:S(2)}) copy-start(f32[2048]{0:T(1024)} %param.20) | copy-start | bytes 24580
  73.8 94.1 %copy-start.7 = (f32[64,2]{0,1:T(2,128)S(1)}, f32[64,2]{0,1:T(2,128)}, u32[]{:S(2)}) copy-start(f32[64,2]{0,1:T(2,128)} %param.22) | copy-start | bytes 1540
